TPU v7x, 256 devices: a whole 4x4x8 slice. The times are simulated.
256 devices in a mesh: ep: 64 (over z, y, core), tp: 4 (over x).
Axes of the slice: x: 4, y: 4, z: 8, core: 2. Of those that a mesh axis runs over, the one named last changes fastest.
Arguments:
- outer_gate: bfloat16 [32768, 2048], P('ep', 'tp'), may hold values from -6 to 6
- inner_gate: bfloat16 [32768, 2048], P('ep', 'tp'), may hold values from -6 to 6
- conv_values: bfloat16 [32768, 2048], P('ep', 'tp'), may hold values from -6 to 6
- conv_taps: bfloat16 [3, 2048], P(None, 'tp'), may hold values from -3 to 3
- out_weight: bfloat16 [2048, 2048], P('tp'), may hold values from -0.125 to 0.125
- moe_input: bfloat16 [32768, 2048], P(('ep', 'tp')), may hold values from -6 to 6
- norm_gain: bfloat16 [2048], replicated, may hold values from 0.099609375 to 1.8984375
- gate_proj: bfloat16 [64, 2048, 1024], P('ep', None, 'tp'), may hold values from -0.125 to 0.125
- up_proj: bfloat16 [64, 2048, 1024], P('ep', None, 'tp'), may hold values from -0.125 to 0.125
- down_proj: bfloat16 [64, 1024, 2048], P('ep', 'tp'), may hold values from -0.1875 to 0.1875
- shared_gate: bfloat16 [2048, 1024], P(None, 'tp'), may hold values from -0.125 to 0.125
- shared_up: bfloat16 [2048, 1024], P(None, 'tp'), may hold values from -0.125 to 0.125
- shared_down: bfloat16 [1024, 2048], P('tp'), may hold values from -0.1875 to 0.1875
- routes: int32 [32768, 2], P('ep'), may hold values from 0 to 63, all different within a row; in each aligned block of 128 rows (0 to 127, 128 to 255, ...) at most 8 rows name the same one
- route_weight: float32 [32768, 2], P('ep'), may hold values from 0.3 to 1.5
Outputs:
- mixer_out: bfloat16 [32768, 2048], P(('ep', 'tp'))
- expert_mix: bfloat16 [32768, 2048], P(('ep', 'tp'))
Inputs may be any that keep to these rules, and one draw needn't show every extreme that they name: `routes`: each row names 2 different experts. In the 128 rows of one device no expert is named more than 8 times, and in every draw some expert is named exactly 8 times in one device's rows.
All inputs are finite; a program needn't handle non-finite values.
Results may differ from a plain program's by a relative error of at most 0.012.
Values may be sent and summed in bfloat16 or wider, within the bound.
No kernel may reach another device: no remote copies, remote signals or barrier semaphores. Data moves between devices by JAX's collectives and lax.ppermute only.
A program may use at most 128 MiB of HBM per device.

v0:
```python
from functools import partial

import jax
import jax.numpy as jnp
from jax import lax
from jax.sharding import PartitionSpec as P

epsilon = 1e-06


def shifted(block, axis, distance):
    devices = range(lax.axis_size(axis))
    route = [(i - distance, i) for i in devices if i - distance in devices]
    return lax.ppermute(block, axis, route)


def from_everyone(array, axis):
    length = lax.axis_size(axis)
    return lax.all_to_all(
        jnp.broadcast_to(array[None], (length, *array.shape)), axis, 0, 0, tiled=True
    )


def joined_along(blocks, dim):
    shape = list(blocks.shape[1:])
    shape[dim] *= blocks.shape[0]
    return jnp.moveaxis(blocks, 0, dim).reshape(shape)


def collect(array, axis, dim):
    blocks = from_everyone(array, axis)
    return joined_along(blocks, dim)


def gather_turned(arrays, axis, dims):
    turned = [jnp.moveaxis(a, dim, 0) for a, dim in zip(arrays, dims)]
    both = jnp.concatenate([t.reshape(len(t), -1) for t in turned], axis=1)
    result, at, outs = (lax.all_gather(both, axis, axis=0, tiled=True), 0, [])
    for t, dim in zip(turned, dims):
        share = result[:, at : at + t[0].size].reshape(-1, *t.shape[1:])
        outs.append(jnp.moveaxis(share, 0, dim))
        at += t[0].size
    return tuple(outs)


def rms_norm(inputs, scales):
    values = inputs.astype(jnp.float32)
    square = jnp.mean(values * values, axis=-1, keepdims=True)
    return (values * lax.rsqrt(square + epsilon) * scales.astype(jnp.float32)).astype(jnp.bfloat16)


def swiglu(inputs, gate_w, up_w):
    gate_term = jnp.dot(inputs, gate_w, preferred_element_type=jnp.float32)
    upward = jnp.dot(inputs, up_w, preferred_element_type=jnp.float32)
    return (jax.nn.silu(gate_term) * upward).astype(jnp.bfloat16)


def slot_table(block_routes, experts, capacity):
    flat_ids = block_routes.reshape(-1)
    onehot = (flat_ids[:, None] == jnp.arange(experts, dtype=jnp.int32)[None, :]).astype(jnp.int32)
    earlier = jnp.cumsum(onehot, axis=0) - onehot
    slot_ids = jnp.sum(earlier * onehot, axis=1)
    targets = flat_ids * capacity + slot_ids
    owners = jnp.arange(flat_ids.shape[0], dtype=jnp.int32) // block_routes.shape[1]
    sources = jnp.zeros((experts * capacity,), jnp.int32).at[targets].set(owners)
    filled = jnp.zeros((experts * capacity,), jnp.bfloat16).at[targets].set(1.0)
    return (sources, filled, targets)


def send_own(normed, own_routes, table_maker, ep_count, capacity):
    sources, filled, own_targets = table_maker(own_routes)
    outgoing = (normed[sources] * filled[:, None]).reshape(ep_count, capacity, normed.shape[1])
    landed = lax.all_to_all(outgoing, "ep", split_axis=0, concat_axis=0, tiled=True)
    return (landed, own_targets)


def per_device(
    outer_gate,
    inner_gate,
    conv_values,
    conv_taps,
    out_weight,
    moe_input,
    norm_gain,
    gate_proj,
    up_proj,
    down_proj,
    shared_gate,
    shared_up,
    shared_down,
    routes,
    route_weight,
):
    tp_count = lax.axis_size("tp")
    ep_count = lax.axis_size("ep")
    my_slot = lax.axis_index("tp")
    group_len = inner_gate.shape[0]
    mix_rows = group_len // tp_count
    channels = inner_gate.shape[1]
    model_width = moe_input.shape[1]
    own_rows = moe_input.shape[0]
    top_count = routes.shape[1]
    capacity = 2 * own_rows * top_count // ep_count
    slot_rows = ep_count * capacity
    reach_rows = conv_taps.shape[0] - 1
    edge_rows = jnp.stack(
        (inner_gate[group_len - reach_rows :], conv_values[group_len - reach_rows :])
    )
    before = shifted(edge_rows, "ep", 1)
    full_gate = jnp.concatenate((before[0], inner_gate), axis=0).astype(jnp.float32)
    full_values = jnp.concatenate((before[1], conv_values), axis=0).astype(jnp.float32)
    product = full_gate * full_values
    tap_values = conv_taps.astype(jnp.float32)
    convolved = tap_values[0] * product[0:group_len]
    for offset in range(1, reach_rows + 1):
        convolved = convolved + tap_values[offset] * product[offset : offset + group_len]
    gate_rows = (outer_gate.astype(jnp.float32) * convolved).astype(jnp.bfloat16)
    gate_rows = gate_rows.reshape(tp_count, mix_rows, channels)
    normed = rms_norm(moe_input, norm_gain)
    group_normed = collect(normed, "tp", 0)
    group_split = group_normed.reshape(tp_count, own_rows, model_width)
    own_weights = lax.dynamic_slice_in_dim(route_weight, my_slot * own_rows, own_rows, 0)
    own_routes = lax.dynamic_slice_in_dim(routes, my_slot * own_rows, own_rows, 0)
    table_maker = partial(slot_table, experts=ep_count, capacity=capacity)
    local_routed = None
    landed, own_targets = send_own(normed, own_routes, table_maker, ep_count, capacity)
    gate_full, up_full, down_full = gather_turned((gate_proj, up_proj, down_proj), "tp", (2, 2, 1))
    hidden = swiglu(landed.reshape(slot_rows, model_width), gate_full[0], up_full[0])
    unit_block = hidden.shape[1] // tp_count
    local_routed = jnp.zeros((slot_rows, model_width), jnp.float32)
    for piece_idx in range(tp_count):
        partial_sum = jnp.dot(
            hidden[:, piece_idx * unit_block : (piece_idx + 1) * unit_block],
            down_full[0, piece_idx * unit_block : (piece_idx + 1) * unit_block],
            preferred_element_type=jnp.float32,
        ).astype(jnp.bfloat16)
        local_routed = local_routed + partial_sum.astype(jnp.float32)
    routed_rows = 0
    expert_block = routed_rows + own_rows
    joint_block = mix_rows + expert_block
    dev_count = joint_block * lax.axis_size("tp") // joint_block
    block_rows = gate_rows
    block_rows = block_rows.reshape(dev_count * mix_rows, channels)
    projected = jnp.dot(block_rows, out_weight, preferred_element_type=jnp.float32)
    shared_in = group_split
    shared_in = shared_in.reshape(dev_count * own_rows, model_width)
    shared_out = jnp.dot(
        swiglu(shared_in, shared_gate, shared_up), shared_down, preferred_element_type=jnp.float32
    )
    shared_out = shared_out.reshape(dev_count, own_rows, model_width)
    combined = jnp.concatenate(
        (projected.reshape(dev_count, mix_rows, model_width), shared_out), axis=1
    )
    summed = lax.psum_scatter(
        combined.reshape(dev_count * joint_block, model_width).astype(jnp.bfloat16),
        "tp",
        scatter_dimension=0,
        tiled=True,
    ).astype(jnp.float32)
    mixer_out = summed[:mix_rows].astype(jnp.bfloat16)
    expert_total = summed[mix_rows:]
    routed_back = local_routed.astype(jnp.bfloat16)
    routed_back = routed_back.reshape(ep_count, capacity, model_width)
    returned = lax.all_to_all(routed_back, "ep", split_axis=0, concat_axis=0, tiled=True).reshape(
        slot_rows, model_width
    )
    picked = returned[own_targets].reshape(own_rows, top_count, model_width).astype(jnp.float32)
    routed = jnp.sum(picked * own_weights[:, :, None], axis=1)
    expert_mix = (expert_total + routed).astype(jnp.bfloat16)
    return (mixer_out, expert_mix)


def solution(mesh):
    return jax.shard_map(
        per_device,
        mesh=mesh,
        in_specs=(
            P("ep", "tp"),
            P("ep", "tp"),
            P("ep", "tp"),
            P(None, "tp"),
            P("tp", None),
            P(("ep", "tp"), None),
            P(),
            P("ep", None, "tp"),
            P("ep", None, "tp"),
            P("ep", "tp", None),
            P(None, "tp"),
            P(None, "tp"),
            P("tp", None),
            P("ep", None),
            P("ep", None),
        ),
        out_specs=(P(("ep", "tp"), None), P(("ep", "tp"), None)),
        check_vma=False,
    )
```

profile of v0, /device:TPU:8, one launch (start us, length us, event | category | flops | bytes accessed | tf_op | source)
XLA Modules:
  0.0 245.1 jit_solution(8007941486165297258)
XLA Ops:
  7.2 1.6 copy.24
  8.9 2.3 copy.25
  11.1 3.0 %pad_maximum_fusion.1 = bf16[256,6144]{1,0:T(8,128)(2,1)} fusion(bf16[256,2048]{1,0:T(8,128)(2,1)} %bitcast.97, bf16[256,2048]{1,0:T(8,128)(2,1)} %bitcast.94, bf16[256,2048]{1,0:T(8,128)(2,1)S(1)} %bitcast.93), kind=kLoop, calls=%fused_computation.11 | loop fusion | flops 9437184 | bytes 6291456 | tf_op jit(solution)/shard_map/concatenate | solution.py:37
  14.1 0.7 copy-done.9
  14.8 0.4 copy-done.2
  15.2 0.2 fusion.8
  15.4 0.2 fusion.10
  15.6 1.6 broadcast_in_dim.8
  17.2 4.5 %all-to-all-start = ((bf16[4,128,2048]{2,1,0:T(8,128)(2,1)}), bf16[4,128,2048]{2,1,0:T(8,128)(2,1)}, u32[]{:S(2)}, u32[]{:S(2)}) async-start(bf16[4,128,2048]{2,1,0:T(8,128)(2,1)} %broadcast_in_dim.8), calls=%async_computation | async-start | bytes 4194304 | tf_op jit(solution)/shard_map/all_to_all | solution.py:19
  21.7 0.7 broadcast_multiply_fusion
  22.5 0.1 eq.29
  22.6 0.1 eq.25
  22.8 0.6 reduce-window.6
  23.4 0.2 slice_reduce_fusion
  23.7 0.1 mul.132
  24.0 1.4 scatter_custom_fusion
  25.4 3.3 %gather_fusion = bf16[512,2048]{1,0:T(8,128)(2,1)} fusion(bf16[128,2048]{1,0:T(8,128)(2,1)S(1)} %fusion.10, s32[1024]{0:T(1024)S(1)} %pad_clamp_fusion.1), kind=kCustom, calls=%fused_computation | custom fusion | bytes 4196352 | tf_op jit(solution)/shard_map/gather | solution.py:72
  28.7 2.2 scatter_custom_fusion.1
  31.0 3.5 %bitcast_multiply_fusion = bf16[64,8,2048]{2,1,0:T(8,128)(2,1)} fusion(bf16[512,2048]{1,0:T(8,128)(2,1)} %gather_fusion, bf16[64,8]{1,0:T(8,128)(2,1)S(1)} %mul.134), kind=kLoop, calls=%fused_computation.21 | loop fusion | flops 1048576 | bytes 4195328 | tf_op jit(solution)/shard_map/mul | solution.py:72
  34.5 26.7 %all-to-all-done = bf16[4,128,2048]{2,1,0:T(8,128)(2,1)} async-done(((bf16[4,128,2048]{2,1,0:T(8,128)(2,1)}), bf16[4,128,2048]{2,1,0:T(8,128)(2,1)}, u32[]{:S(2)}, u32[]{:S(2)}) %all-to-all-start) | async-done | bytes 2097184 | tf_op jit(solution)/shard_map/all_to_all | solution.py:19
  61.2 13.8 %all-to-all-start.1 = ((bf16[64,8,2048]{2,1,0:T(8,128)(2,1)}), bf16[64,8,2048]{2,1,0:T(8,128)(2,1)}, u32[]{:S(2)}, u32[]{:S(2)}) async-start(bf16[64,8,2048]{2,1,0:T(8,128)(2,1)} %bitcast_multiply_fusion), calls=%async_computation.2 | async-start | bytes 4194304 | tf_op jit(solution)/shard_map/all_to_all | solution.py:73
  75.1 2.3 collective-permute-start
  77.5 3.1 %collective-permute-done = bf16[2,2,512]{2,1,0:T(2,128)(2,1)S(1)} collective-permute-done((bf16[2,2,512]{2,1,0:T(2,128)(2,1)S(1)}, bf16[2,2,512]{2,1,0:T(2,128)(2,1)S(1)}, u32[]{:S(2)}, u32[]{:S(2)}) %collective-permute-start) | collective-permute-done | bytes 4128 | tf_op jit(solution)/shard_map/ppermute | solution.py:14
  80.6 0.2 convert_multiply_fusion.2
  80.9 2.8 %convolution_convert_fusion.5 = bf16[512,2048]{1,0:T(8,128)(2,1)} fusion(bf16[512,2048]{1,0:T(8,128)(2,1)S(1)} %copy-done, f32[514,512]{1,0:T(8,128)S(1)} %convert_multiply_fusion.2, bf16[512,512]{1,0:T(8,128)(2,1)S(1)} %copy-done.12, f32[512]{0:T(512)S(1)} %bitcast.104, f32[512]{0:T(512)S(1)} %bitcast.103, f32[512]{0:T(512)S(1)} %bitcast.102), kind=kOutput, calls=%fused_computation.17 | convolution fusion | flops 1076887552 | bytes 7870464 | tf_op jit(solution)/shard_map/dot_general | solution.py:144
  83.6 3.2 %fusion.39 = f32[512,256]{1,0:T(8,128)} fusion(bf16[512,2048]{1,0:T(8,128)(2,1)} %bitcast.8, bf16[2048,256]{1,0:T(8,128)(2,1)S(1)} %copy-done.10), kind=kOutput, calls=%fused_computation.89 | convolution fusion | flops 536870912 | bytes 3670016 | tf_op jit(solution)/shard_map/dot_general | solution.py:53
  86.9 5.8 %convolution_convert_fusion.4 = bf16[512,2048]{1,0:T(8,128)(2,1)} fusion(bf16[256,2048]{1,0:T(8,128)(2,1)S(1)} %copy-done.11, bf16[512,2048]{1,0:T(8,128)(2,1)} %bitcast.8, bf16[2048,256]{1,0:T(8,128)(2,1)} %param.26, f32[512,256]{1,0:T(8,128)} %fusion.39), kind=kOutput, calls=%fused_computation.16 | convolution fusion | flops 1075576832 | bytes 6815744 | tf_op jit(solution)/shard_map/dot_general | solution.py:147
  92.7 4.2 %pad_maximum_fusion = bf16[4,256,2048]{2,1,0:T(8,128)(2,1)} fusion(bf16[4,128,2048]{2,1,0:T(8,128)(2,1)} %bitcast.96, bf16[4,128,2048]{2,1,0:T(8,128)(2,1)S(1)} %bitcast.95), kind=kLoop, calls=%fused_computation.9 | loop fusion | flops 8388608 | bytes 8388608 | tf_op jit(solution)/shard_map/concatenate | solution.py:151
  96.9 29.3 %all-to-all-done.1 = bf16[64,8,2048]{2,1,0:T(8,128)(2,1)} async-done(((bf16[64,8,2048]{2,1,0:T(8,128)(2,1)}), bf16[64,8,2048]{2,1,0:T(8,128)(2,1)}, u32[]{:S(2)}, u32[]{:S(2)}) %all-to-all-start.1) | async-done | bytes 2097184 | tf_op jit(solution)/shard_map/all_to_all | solution.py:73
  126.1 23.3 %all-gather.2.cloned.1.call-done = bf16[1024,6144]{1,0:T(8,128)(2,1)} async-done(((bf16[256,6144]{1,0:T(8,128)(2,1)}), bf16[1024,6144]{1,0:T(8,128)(2,1)}) %all-gather.2.cloned.1.call-update) | async-done | bytes 12582928 | tf_op jit(solution)/shard_map/all_gather | solution.py:38
  149.4 5.3 %fusion.1 = f32[512,1024]{1,0:T(8,128)S(1)} fusion(bf16[1024,6144]{1,0:T(8,128)(2,1)} %all-gather.2.cloned.1.call-done, bf16[64,8,2048]{2,1,0:T(8,128)(2,1)} %all-to-all-done.1), kind=kOutput, calls=%fused_computation.8 | convolution fusion | flops 2147483648 | bytes 8388608 | tf_op jit(solution)/shard_map/dot_general | solution.py:53
  154.7 1.1 copy-done.4
  155.8 0.6 slice_bitcast_fusion
  156.4 4.1 %multiply_convert_fusion = bf16[512,1024]{1,0:T(8,128)(2,1)S(1)} fusion(f32[512,1024]{1,0:T(8,128)S(1)} %fusion.1, bf16[1024,6144]{1,0:T(8,128)(2,1)S(1)} %copy-done.4, bf16[64,8,2048]{2,1,0:T(8,128)(2,1)} %all-to-all-done.1), kind=kOutput, calls=%fused_computation.23 | convolution fusion | flops 2150629376 | bytes 9437184 | tf_op jit(solution)/shard_map/dot_general | solution.py:54
  160.5 0.7 convolution_convert_fusion.2
  161.3 0.7 convolution_convert_fusion.1
  162.0 0.7 convolution_convert_fusion
  162.7 2.6 %fusion.2 = bf16[64,8,2048]{2,1,0:T(8,128)(2,1)} fusion(bf16[512,2048]{1,0:T(8,128)(2,1)S(1)} %convolution_convert_fusion, bf16[512,2048]{1,0:T(8,128)(2,1)S(1)} %convolution_convert_fusion.1, bf16[512,2048]{1,0:T(8,128)(2,1)S(1)} %convolution_convert_fusion.2, bf16[1,1024,2048]{2,1,0:T(8,128)(2,1)S(1)} %slice_bitcast_fusion, ...), kind=kOutput, calls=%fused_computation.18 | convolution fusion | flops 546308096 | bytes 9699328 | tf_op jit(solution)/shard_map/dot_general | solution.py:132
  165.4 12.1 %all-to-all-start.2 = ((bf16[64,8,2048]{2,1,0:T(8,128)(2,1)}), bf16[64,8,2048]{2,1,0:T(8,128)(2,1)S(1)}, u32[]{:S(2)}, u32[]{:S(2)}) async-start(bf16[64,8,2048]{2,1,0:T(8,128)(2,1)} %fusion.2), calls=%async_computation.3 | async-start | bytes 4194304 | tf_op jit(solution)/shard_map/all_to_all | solution.py:164
  177.5 0.7 constant_dynamic-slice_fusion
  178.1 0.1 copy.26
  178.3 24.4 %reduce-scatter.2.cloned.1.call-done = bf16[256,2048]{1,0:T(8,128)(2,1)} async-done(((bf16[1024,2048]{1,0:T(8,128)(2,1)}), bf16[256,2048]{1,0:T(8,128)(2,1)}) %reduce-scatter.2.cloned.1.call-update) | async-done | bytes 1048592 | tf_op jit(solution)/shard_map/reduce_scatter | solution.py:154
  202.7 1.9 slice.117
  204.5 24.2 %all-to-all-done.2 = bf16[64,8,2048]{2,1,0:T(8,128)(2,1)S(1)} async-done(((bf16[64,8,2048]{2,1,0:T(8,128)(2,1)}), bf16[64,8,2048]{2,1,0:T(8,128)(2,1)S(1)}, u32[]{:S(2)}, u32[]{:S(2)}) %all-to-all-start.2) | async-done | bytes 2097184 | tf_op jit(solution)/shard_map/all_to_all | solution.py:164
  228.7 1.4 gather_fusion.1
  230.1 2.4 reshape.113
  232.4 4.9 %multiply_reduce_fusion = f32[128,2048]{1,0:T(8,128)S(1)} fusion(f32[128,2,2048]{2,1,0:T(2,128)} %reshape.113, f32[128,2]{1,0:T(8,128)S(1)} %copy.26), kind=kLoop, calls=%fused_computation.22 | loop fusion | flops 786432 | bytes 3146752 | tf_op jit(solution)/shard_map/reduce_sum | solution.py:168
  237.3 0.9 add_convert_fusion.1
  (46 shorter events, 0.7 us)
Async XLA Ops:
  7.2 73.7 %copy-start = (bf16[512,2048]{1,0:T(8,128)(2,1)S(1)}, bf16[512,2048]{1,0:T(8,128)(2,1)}, u32[]{:S(2)}) copy-start(bf16[512,2048]{1,0:T(8,128)(2,1)} %param.19) | copy-start | bytes 6291460
  7.2 142.2 %all-gather.2.cloned.1.call-start = ((), (), s32[]{:S(2)}) async-start(), calls=%async_computation.5 | async-start | bytes 15728640 | tf_op jit(solution)/shard_map/all_gather | solution.py:38
  14.1 0.7 copy-start.9
  14.1 1.1 copy-start.2
  17.2 44.0 %all-to-all-start = ((bf16[4,128,2048]{2,1,0:T(8,128)(2,1)}), bf16[4,128,2048]{2,1,0:T(8,128)(2,1)}, u32[]{:S(2)}, u32[]{:S(2)}) async-start(bf16[4,128,2048]{2,1,0:T(8,128)(2,1)} %broadcast_in_dim.8), calls=%async_computation | async-start | bytes 4194304 | tf_op jit(solution)/shard_map/all_to_all | solution.py:19
  34.5 40.5 %copy-start.6 = (bf16[512,512]{1,0:T(8,128)(2,1)S(1)}, bf16[512,512]{1,0:T(8,128)(2,1)}, u32[]{:S(2)}) copy-start(bf16[512,512]{1,0:T(8,128)(2,1)} %param.16) | copy-start | bytes 1572868
  34.5 40.5 %copy-start.7 = (bf16[512,512]{1,0:T(8,128)(2,1)S(1)}, bf16[512,512]{1,0:T(8,128)(2,1)}, u32[]{:S(2)}) copy-start(bf16[512,512]{1,0:T(8,128)(2,1)} %param.17) | copy-start | bytes 1572868
  34.5 42.9 %copy-start.8 = (bf16[3,512]{1,0:T(4,128)(2,1)S(1)}, bf16[3,512]{1,0:T(4,128)(2,1)}, u32[]{:S(2)}) copy-start(bf16[3,512]{1,0:T(4,128)(2,1)} %param.18) | copy-start | bytes 9220
  61.2 65.0 %all-to-all-start.1 = ((bf16[64,8,2048]{2,1,0:T(8,128)(2,1)}), bf16[64,8,2048]{2,1,0:T(8,128)(2,1)}, u32[]{:S(2)}, u32[]{:S(2)}) async-start(bf16[64,8,2048]{2,1,0:T(8,128)(2,1)} %bitcast_multiply_fusion), calls=%async_computation.2 | async-start | bytes 4194304 | tf_op jit(solution)/shard_map/all_to_all | solution.py:73
  75.0 127.7 %reduce-scatter.2.cloned.1.call-start = ((), (), s32[]{:S(2)}) async-start(), calls=%async_computation.4 | async-start | bytes 5242880 | tf_op jit(solution)/shard_map/reduce_scatter | solution.py:154
  75.1 5.8 %copy-start.12 = (bf16[512,512]{1,0:T(8,128)(2,1)S(1)}, bf16[512,512]{1,0:T(8,128)(2,1)}, u32[]{:S(2)}) copy-start(bf16[512,512]{1,0:T(8,128)(2,1)} %param.15) | copy-start | bytes 1572868
  75.1 5.5 %collective-permute-start = (bf16[2,2,512]{2,1,0:T(2,128)(2,1)S(1)}, bf16[2,2,512]{2,1,0:T(2,128)(2,1)S(1)}, u32[]{:S(2)}, u32[]{:S(2)}) collective-permute-start(bf16[2,2,512]{2,1,0:T(2,128)(2,1)S(1)} %pad_maximum_fusion.2), channel_id=1, source_target_pairs={{0,4},{4,8},{8,12},{12,16},{16,20},{20,24},{24,28},{28,32},{32,36}... | collective-permute-start | bytes 12296 | tf_op jit(solution)/shard_map/ppermute | solution.py:14
  80.9 2.8 %copy-start.10 = (bf16[2048,256]{1,0:T(8,128)(2,1)S(1)}, bf16[2048,256]{1,0:T(8,128)(2,1)}, u32[]{:S(2)}) copy-start(bf16[2048,256]{1,0:T(8,128)(2,1)} %param.25) | copy-start | bytes 3145732
  83.6 3.2 %copy-start.11 = (bf16[256,2048]{1,0:T(8,128)(2,1)S(1)}, bf16[256,2048]{1,0:T(8,128)(2,1)}, u32[]{:S(2)}) copy-start(bf16[256,2048]{1,0:T(8,128)(2,1)} %param.27) | copy-start | bytes 3145732
  86.9 5.8 %copy-start.3 = (bf16[512,2048]{1,0:T(8,128)(2,1)S(1)}, bf16[512,2048]{1,0:T(8,128)(2,1)}, u32[]{:S(2)}) copy-start(bf16[512,2048]{1,0:T(8,128)(2,1)} %convolution_convert_fusion.5) | copy-start | bytes 6291460
  149.4 6.4 %copy-start.4 = (bf16[1024,6144]{1,0:T(8,128)(2,1)S(1)}, bf16[1024,6144]{1,0:T(8,128)(2,1)}, u32[]{:S(2)}) copy-start(bf16[1024,6144]{1,0:T(8,128)(2,1)} %all-gather.2.cloned.1.call-done) | copy-start | bytes 37748740
  165.4 63.3 %all-to-all-start.2 = ((bf16[64,8,2048]{2,1,0:T(8,128)(2,1)}), bf16[64,8,2048]{2,1,0:T(8,128)(2,1)S(1)}, u32[]{:S(2)}, u32[]{:S(2)}) async-start(bf16[64,8,2048]{2,1,0:T(8,128)(2,1)} %fusion.2), calls=%async_computation.3 | async-start | bytes 4194304 | tf_op jit(solution)/shard_map/all_to_all | solution.py:164
  230.1 8.2 %copy-start.1 = (bf16[512,2048]{1,0:T(8,128)(2,1)S(1)}, bf16[512,2048]{1,0:T(8,128)(2,1)}, u32[]{:S(2)}) copy-start(bf16[512,2048]{1,0:T(8,128)(2,1)} %param.19) | copy-start | bytes 6291460
  232.4 4.9 %copy-start.5 = (bf16[256,2048]{1,0:T(8,128)(2,1)S(1)}, bf16[256,2048]{1,0:T(8,128)(2,1)}, u32[]{:S(2)}) copy-start(bf16[256,2048]{1,0:T(8,128)(2,1)} %reduce-scatter.2.cloned.1.call-done) | copy-start | bytes 3145732
Sparse Core Ops, SparseCore 0:
  14.3 135.0 all-gather.1
  151.9 50.6 reduce-scatter.1
where the time goes:
time: 246 us; the launch traced here: 245 us
  waiting for transfers between devices  131 us (53%)
  starting transfers between devices  32.8 us (13%)
  matrix products  26.1 us (11%)
  local copies, waits for them, and re-layouts  22.4 us (9%)
  other arithmetic  18.6 us (8%)
  between operations  14.3 us (6%)
    all_to_all x1, waiting for transfers between devices, send_own(): lax.all_to_all(outgoing, 'ep', split_axis=0, concat_axis=0, tiled=True)  29.3 us
    all_to_all x1, waiting for transfers between devices, from_everyone(): lax.all_to_all(jnp.broadcast_to(array[None], (length, *array.shape)), axi...  26.7 us
    reduce_scatter x1, waiting for transfers between devices, per_device(): lax.psum_scatter(combined.reshape(dev_count * joint_block, model_width).a...  24.4 us
    all_to_all x1, waiting for transfers between devices, per_device(): lax.all_to_all(routed_back, 'ep', split_axis=0, concat_axis=0, tiled=True)  24.2 us
    all_gather x1, waiting for transfers between devices, gather_turned(): result, at, outs = (lax.all_gather(both, axis, axis=0, tiled=True), 0, [])  23.3 us
    all_to_all x1, starting transfers between devices, send_own(): lax.all_to_all(outgoing, 'ep', split_axis=0, concat_axis=0, tiled=True)  13.8 us
    all_to_all x1, starting transfers between devices, per_device(): lax.all_to_all(routed_back, 'ep', split_axis=0, concat_axis=0, tiled=True)  12.1 us
    dot_general x2, matrix products, swiglu(): gate_term = jnp.dot(inputs, gate_w, preferred_element_type=jnp.float32)  8.57 us
  transfers between devices with their start and end apart: 6, of which 6 were waited for; matrix products, arithmetic and copies ran while one was open for 20% of the time, Pallas kernels for 0%

commit v1 on v0

v1 whole, which is shorter than its diff:
```python
import jax
import jax.numpy as jnp
from jax import lax
from jax.experimental import pallas as pl
from jax.experimental.pallas import tpu as pltpu
from jax.sharding import PartitionSpec as P


epsilon = 1e-06


def turn(array, axis, distance):
    size = lax.axis_size(axis)
    return lax.ppermute(array, axis, [(i, (i + distance) % size) for i in range(size)])


def shifted(block, axis, distance):
    devices = range(lax.axis_size(axis))
    route = [(i - distance, i) for i in devices if i - distance in devices]
    return lax.ppermute(block, axis, route)


def exchanged(blocks):
    return lax.all_to_all(blocks, "ep", 0, 0, tiled=True)


def both(first, second):
    return first.astype(jnp.float32) + second.astype(jnp.float32)


def after(value, *others):
    return lax.optimization_barrier((value, *others))[0]


def rms_norm(inputs, scales):
    values = inputs.astype(jnp.float32)
    square = jnp.mean(values * values, axis=-1, keepdims=True)
    return (values * lax.rsqrt(square + epsilon) * scales.astype(jnp.float32)).astype(jnp.bfloat16)


def dot(left, right):
    return jnp.dot(left, right, preferred_element_type=jnp.float32)


def swiglu(inputs, gate_w, up_w):
    return (jax.nn.silu(dot(inputs, gate_w)) * dot(inputs, up_w)).astype(jnp.bfloat16)


def hidden_kernel(*refs):
    count = (len(refs) - 6) // 2
    x_hbm, weights, out = refs[0], refs[1 : 1 + 2 * count], refs[1 + 2 * count]
    x, held, x_sem, sems = refs[2 + 2 * count :]
    copies = [pltpu.make_async_copy(w, held.at[i], sems.at[i]) for i, w in enumerate(weights)]
    first = pltpu.make_async_copy(x_hbm, x, x_sem.at[0])
    first.start()
    for copy in copies:
        copy.start()
    first.wait()
    units = out.shape[1] // count
    for i in range(count):
        copies[2 * i].wait()
        gate_term = dot(x[...], held[2 * i])
        copies[2 * i + 1].wait()
        upward = dot(x[...], held[2 * i + 1])
        out[:, i * units : (i + 1) * units] = (jax.nn.silu(gate_term) * upward).astype(out.dtype)


def hidden_units(rows, pairs):
    weights = [w for pair in pairs for w in pair]
    anywhere = pl.BlockSpec(memory_space=pl.ANY)
    return pl.pallas_call(
        hidden_kernel,
        out_shape=jax.ShapeDtypeStruct((rows.shape[0], len(pairs) * weights[0].shape[1]), rows.dtype),
        in_specs=[anywhere] * (1 + len(weights)),
        out_specs=pl.BlockSpec(memory_space=pltpu.VMEM),
        scratch_shapes=[
            pltpu.VMEM(rows.shape, rows.dtype),
            pltpu.VMEM((len(weights), *weights[0].shape), rows.dtype),
            pltpu.SemaphoreType.DMA((1,)),
            pltpu.SemaphoreType.DMA((len(weights),)),
        ],
        name="hidden_units",
    )(rows, *weights)


def down_kernel(*refs):
    count = len(refs) - 6
    hidden_hbm, blocks, out = refs[0], refs[1 : 1 + count], refs[1 + count]
    hidden, held, sums, sems = refs[2 + count :]
    starts = [0]
    for block in blocks:
        starts.append(starts[-1] + block.shape[0])
    first = pltpu.make_async_copy(hidden_hbm, hidden, sems.at[0])
    first.start()
    copies = []
    for i, block in enumerate(blocks):
        place = held.at[pl.ds(starts[i], block.shape[0])]
        copies.append(pltpu.make_async_copy(block, place, sems.at[1 + i]))
        copies[-1].start()
    first.wait()
    for copy in copies:
        copy.wait()
    tiles, _, width = sums.shape
    stores = []
    for t in range(tiles):
        cols = slice(t * width, (t + 1) * width)
        sums[t] = dot(hidden[...], held[:, cols]).astype(sums.dtype)
        place = out.at[:, pl.ds(t * width, width)]
        stores.append(pltpu.make_async_copy(sums.at[t], place, sems.at[1 + count + t]))
        stores[-1].start()
    for store in stores:
        store.wait()


def down_product(hidden, blocks, tiles=4):
    units = sum(block.shape[0] for block in blocks)
    width = blocks[0].shape[1]
    anywhere = pl.BlockSpec(memory_space=pl.ANY)
    return pl.pallas_call(
        down_kernel,
        out_shape=jax.ShapeDtypeStruct((hidden.shape[0], width), hidden.dtype),
        in_specs=[anywhere] * (1 + len(blocks)),
        out_specs=anywhere,
        scratch_shapes=[
            pltpu.VMEM(hidden.shape, hidden.dtype),
            pltpu.VMEM((units, width), hidden.dtype),
            pltpu.VMEM((tiles, hidden.shape[0], width // tiles), hidden.dtype),
            pltpu.SemaphoreType.DMA((1 + len(blocks) + tiles,)),
        ],
        name="down_product",
    )(hidden, *blocks)


def slots_of(block_routes, experts, capacity):
    tokens = block_routes.shape[0]
    hits = block_routes[:, :, None] == jnp.arange(experts, dtype=jnp.int32)
    hits = hits.astype(jnp.bfloat16)
    rows = lax.broadcasted_iota(jnp.int32, (tokens, tokens), 0)
    cols = lax.broadcasted_iota(jnp.int32, (tokens, tokens), 1)
    earlier = dot((cols < rows).astype(jnp.bfloat16), hits.sum(axis=1))
    rank = jnp.sum(earlier[:, None, :] * hits.astype(jnp.float32), axis=2)
    return block_routes * capacity + rank.astype(jnp.int32)


def per_device(
    outer_gate,
    inner_gate,
    conv_values,
    conv_taps,
    out_weight,
    moe_input,
    norm_gain,
    gate_proj,
    up_proj,
    down_proj,
    shared_gate,
    shared_up,
    shared_down,
    routes,
    route_weight,
):
    tp_count = lax.axis_size("tp")
    ep_count = lax.axis_size("ep")
    my_slot = lax.axis_index("tp")
    group_len = inner_gate.shape[0]
    mix_rows = group_len // tp_count
    model_width = moe_input.shape[1]
    own_rows = moe_input.shape[0]
    top_count = routes.shape[1]
    capacity = 2 * own_rows * top_count // ep_count
    slot_rows = ep_count * capacity
    reach_rows = conv_taps.shape[0] - 1
    half_units = down_proj.shape[1] // 2
    half_rows = own_rows // 2

    gate_o, up_o, down_o = gate_proj[0], up_proj[0], down_proj[0]
    gate_l = turn(gate_o, "tp", 1)
    up_r = turn(up_o, "tp", -1)
    up_l = turn(up_o, "tp", 1)
    gate_r = turn(gate_o, "tp", -1)
    gate_p = turn(gate_l, "tp", 1)
    up_p = turn(up_r, "tp", -1)

    edge_rows = jnp.stack(
        (inner_gate[group_len - reach_rows :], conv_values[group_len - reach_rows :])
    )
    before = shifted(edge_rows, "ep", 1)

    normed = rms_norm(moe_input, norm_gain)
    own_weights = lax.dynamic_slice_in_dim(route_weight, my_slot * own_rows, own_rows, 0)
    own_routes = lax.dynamic_slice_in_dim(routes, my_slot * own_rows, own_rows, 0)
    slots = slots_of(own_routes, ep_count, capacity)
    slot_ids = lax.broadcasted_iota(jnp.int32, (slot_rows, own_rows), 0)
    chosen = (slot_ids == slots[:, 0][None]) | (slot_ids == slots[:, 1][None])
    outgoing = dot(chosen.astype(jnp.bfloat16), normed).astype(jnp.bfloat16)
    landed = exchanged(outgoing.reshape(ep_count, capacity, model_width))
    landed = landed.reshape(slot_rows, model_width)

    down_s = after(down_o, gate_l, up_r)
    down_l = turn(down_s, "tp", 1)
    down_r = turn(down_s, "tp", -1)

    full_gate = jnp.concatenate((before[0], inner_gate), axis=0).astype(jnp.float32)
    full_values = jnp.concatenate((before[1], conv_values), axis=0).astype(jnp.float32)
    product = full_gate * full_values
    tap_values = conv_taps.astype(jnp.float32)
    convolved = tap_values[0] * product[0:group_len]
    for offset in range(1, reach_rows + 1):
        convolved = convolved + tap_values[offset] * product[offset : offset + group_len]
    gate_rows = (outer_gate.astype(jnp.float32) * convolved).astype(jnp.bfloat16)
    mix = []
    for step in range(tp_count):
        place = lax.rem(my_slot + step, tp_count)
        rows = lax.dynamic_slice_in_dim(gate_rows, place * mix_rows, mix_rows, 0)
        mix.append(dot(rows, out_weight).astype(jnp.bfloat16))

    def shared_part(rows):
        return dot(swiglu(rows, shared_gate, shared_up), shared_down).astype(jnp.bfloat16)

    shared_own = shared_part(normed)

    landed = after(landed, shared_own, *mix)
    pairs = ((gate_o, up_o), (gate_l, up_l), (gate_r, up_r), (gate_p, up_p))
    hidden = hidden_units(landed, pairs)
    down_l, down_r = after(down_l, hidden), after(down_r, hidden)
    down_p0 = turn(down_l[:half_units], "tp", 1)
    down_p1 = turn(down_r[half_units:], "tp", -1)
    total = down_product(hidden, (down_o, down_l, down_r, down_p0, down_p1))
    returned = exchanged(total.reshape(ep_count, capacity, model_width))
    returned = returned.reshape(slot_rows, model_width)

    normed_s = after(normed, down_l, down_r)
    normed_l = turn(normed_s, "tp", 1)
    normed_r = turn(normed_s, "tp", -1)

    far, left = after(mix[2], total), after(mix[3], total)
    far = turn(far, "tp", 1)
    from_r = turn(left, "tp", -1)
    normed_l, normed_r = after(normed_l, total), after(normed_r, total)
    normed_p0 = turn(normed_l[:half_rows], "tp", 1)
    normed_p1 = turn(normed_r[half_rows:], "tp", -1)
    normed_p = jnp.concatenate((normed_p0, normed_p1), axis=0)
    from_l = turn(both(mix[1], far).astype(jnp.bfloat16), "tp", 1)
    mixer_out = (both(mix[0], from_l) + from_r.astype(jnp.float32)).astype(jnp.bfloat16)

    share_r, share_l = shared_part(normed_r), shared_part(normed_l)
    far = turn(shared_part(normed_p), "tp", -1)
    from_l = turn(share_r, "tp", 1)
    from_r = turn(both(share_l, far).astype(jnp.bfloat16), "tp", -1)
    shared_total = both(shared_own, from_l) + from_r.astype(jnp.float32)

    slot_ids = lax.broadcasted_iota(jnp.int32, (own_rows, slot_rows), 1)
    routed = shared_total
    for choice in range(top_count):
        picks = (slot_ids == slots[:, choice][:, None]).astype(jnp.bfloat16)
        routed = routed + dot(picks, returned) * own_weights[:, choice][:, None]
    return (mixer_out, routed.astype(jnp.bfloat16))


def solution(mesh):
    return jax.shard_map(
        per_device,
        mesh=mesh,
        in_specs=(
            P("ep", "tp"),
            P("ep", "tp"),
            P("ep", "tp"),
            P(None, "tp"),
            P("tp", None),
            P(("ep", "tp"), None),
            P(),
            P("ep", None, "tp"),
            P("ep", None, "tp"),
            P("ep", "tp", None),
            P(None, "tp"),
            P(None, "tp"),
            P("tp", None),
            P("ep", None),
            P("ep", None),
        ),
        out_specs=(P(("ep", "tp"), None), P(("ep", "tp"), None)),
        check_vma=False,
    )
```

time: 246 us -> 243 us (0.988)
  Pallas kernels: 0 us -> 20.4 us
  starting transfers between devices: 32.8 us -> 49.4 us
  between operations: 14.3 us -> 0.95 us
  local copies, waits for them, and re-layouts: 22.4 us -> 9.33 us
  waiting for transfers between devices: 131 us -> 120 us
  other arithmetic: 18.6 us -> 10.3 us
  matrix products: 26.1 us -> 31.2 us
    ppermute x0 -> x20, waiting for transfers between devices: none -> 120 us  [turn(): lax.ppermute(array, axis, [(i, (i + distance) % size) for i in range(size)])]
    all_to_all x3 -> x2, waiting for transfers between devices: 80.1 us -> 0.01 us  [exchanged(): return lax.all_to_all(blocks, 'ep', 0, 0, tiled=True)]
    ppermute x0 -> x20, starting transfers between devices: none -> 24.6 us  [turn(): lax.ppermute(array, axis, [(i, (i + distance) % size) for i in range(size)])]
    reduce_scatter x1 -> x0, waiting for transfers between devices: 24.4 us -> none  [per_device(): lax.psum_scatter(combined.reshape(dev_count * joint_block, model_width).a...]
    all_gather x1 -> x0, waiting for transfers between devices: 23.3 us -> none  [gather_turned(): result, at, outs = (lax.all_gather(both, axis, axis=0, tiled=True), 0, [])]
    pallas_call x0 -> x2, Pallas kernels: none -> 20.4 us  [the longest x1 14.7 us: hidden_units(): pl.pallas_call(hidden_kernel, out_shape=jax.ShapeDtypeStruct((rows.shape[...]
    all_to_all x3 -> x2, starting transfers between devices: 30.4 us -> 22.9 us  [exchanged(): return lax.all_to_all(blocks, 'ep', 0, 0, tiled=True)]
    concatenate x2 -> x0, other arithmetic: 7.16 us -> none  [the longest x1 4.17 us: per_device(): jnp.concatenate((projected.reshape(dev_count, mix_rows, model_width), sha...]
  transfers between devices with their start and end apart: 6 -> 23, of which waited for: 6 -> 8; matrix products, arithmetic and copies ran while one was open for 20% -> 15% of each run, Pallas kernels for 0% -> 6%
where the time goes in v1:
time: 243 us; the launch traced here: 241 us
  waiting for transfers between devices  120 us (49%)
  starting transfers between devices  49.4 us (20%)
  matrix products  31.2 us (13%)
  Pallas kernels  20.4 us (8%)
  other arithmetic  10.3 us (4%)
  local copies, waits for them, and re-layouts  9.33 us (4%)
    ppermute x20, waiting for transfers between devices, turn(): lax.ppermute(array, axis, [(i, (i + distance) % size) for i in range(size)])  120 us
    dot_general x16, matrix products, dot(): return jnp.dot(left, right, preferred_element_type=jnp.float32)  31.2 us
    ppermute x20, starting transfers between devices, turn(): lax.ppermute(array, axis, [(i, (i + distance) % size) for i in range(size)])  24.6 us
    all_to_all x2, starting transfers between devices, exchanged(): return lax.all_to_all(blocks, 'ep', 0, 0, tiled=True)  22.9 us
    pallas_call x1, Pallas kernels, hidden_units(): pl.pallas_call(hidden_kernel, out_shape=jax.ShapeDtypeStruct((rows.shape[...  14.7 us
    pallas_call x1, Pallas kernels, down_product(): pl.pallas_call(down_kernel, out_shape=jax.ShapeDtypeStruct((hidden.shape[...  5.73 us
  transfers between devices with their start and end apart: 23, of which 8 were waited for; matrix products, arithmetic and copies ran while one was open for 15% of the time, Pallas kernels for 6%

profile of v1, /device:TPU:8, one launch (start us, length us, event | category | flops | bytes accessed | tf_op | source)
XLA Modules:
  0.0 241.5 jit_solution(2171259322901063107)
XLA Ops:
  0.7 0.8 constant_dynamic-slice_fusion.1
  3.1 1.2 fusion.5
  4.3 1.2 fusion.7
  5.6 0.8 copy-done.2
  6.4 2.0 fusion
  8.4 12.4 %all-to-all-start = ((bf16[64,8,2048]{2,1,0:T(8,128)(2,1)}), bf16[64,8,2048]{2,1,0:T(8,128)(2,1)}, u32[]{:S(2)}, u32[]{:S(2)}) async-start(bf16[64,8,2048]{2,1,0:T(8,128)(2,1)} %fusion), calls=%async_computation | async-start | bytes 4194304 | tf_op jit(solution)/shard_map/all_to_all | solution.py:24
  20.8 2.8 %collective-permute-start.4 = (bf16[2048,256]{1,0:T(8,128)(2,1)}, bf16[2048,256]{1,0:T(8,128)(2,1)}, u32[]{:S(2)}, u32[]{:S(2)}) collective-permute-start(bf16[2048,256]{1,0:T(8,128)(2,1)} %bitcast.63), channel_id=1, source_target_pairs={{0,3},{1,0},{2,1},{3,2},{4,7},{5,4},{6,5},{7,6},{8,11},{9,8},{10,9... | collective-permute-start | bytes 3145736 | tf_op jit(solution)/shard_map/ppermute | solution.py:14
  24.4 2.5 %collective-permute-start.3 = (bf16[2048,256]{1,0:T(8,128)(2,1)}, bf16[2048,256]{1,0:T(8,128)(2,1)}, u32[]{:S(2)}, u32[]{:S(2)}) collective-permute-start(bf16[2048,256]{1,0:T(8,128)(2,1)} %bitcast.61), channel_id=1, source_target_pairs={{0,3},{1,0},{2,1},{3,2},{4,7},{5,4},{6,5},{7,6},{8,11},{9,8},{10,9... | collective-permute-start | bytes 3145736 | tf_op jit(solution)/shard_map/ppermute | solution.py:14
  27.6 1.9 collective-permute-start
  29.6 1.7 fusion.51
  31.3 3.0 %convolution_convert_fusion.5 = bf16[128,2048]{1,0:T(8,128)(2,1)} fusion(bf16[256,2048]{1,0:T(8,128)(2,1)S(1)} %copy-done.1, bf16[128,2048]{1,0:T(8,128)(2,1)} %copy-done.2, bf16[2048,256]{1,0:T(8,128)(2,1)} %param.26, f32[128,256]{1,0:T(8,128)S(1)} %fusion.51), kind=kOutput, calls=%fused_computation.9 | convolution fusion | flops 268894208 | bytes 3276800 | tf_op jit(solution)/shard_map/dot_general | solution.py:42
  34.4 1.5 convert_multiply_fusion.2
  36.3 36.2 %collective-permute-done.1.refs_3_ = bf16[2048,256]{1,0:T(8,128)(2,1)} collective-permute-done((bf16[2048,256]{1,0:T(8,128)(2,1)}, bf16[2048,256]{1,0:T(8,128)(2,1)}, u32[]{:S(2)}, u32[]{:S(2)}) %collective-permute-start.1) | collective-permute-done | bytes 1048608 | tf_op jit(solution)/shard_map/ppermute | solution.py:14
  72.5 2.0 collective-permute-start.7
  74.6 3.2 %collective-permute-start.6 = (bf16[2048,256]{1,0:T(8,128)(2,1)}, bf16[2048,256]{1,0:T(8,128)(2,1)}, u32[]{:S(2)}, u32[]{:S(2)}) collective-permute-start(bf16[2048,256]{1,0:T(8,128)(2,1)} %collective-permute-done.4.refs_6_), channel_id=1, source_target_pairs={{0,3},{1,0},{2,1},{3,2},{4,7},{5,4},{6,5},{7,6},{8,11},{9,8},{10,9... | collective-permute-start | bytes 3145736 | tf_op jit(solution)/shard_map/ppermute | solution.py:14
  77.8 1.2 convolution_convert_fusion.6
  79.0 1.2 convolution_convert_fusion.7
  80.3 1.2 convolution_convert_fusion.4
  81.5 1.2 convolution_convert_fusion.8
  82.8 37.8 %collective-permute-done.5.refs_7_ = bf16[2048,256]{1,0:T(8,128)(2,1)} collective-permute-done((bf16[2048,256]{1,0:T(8,128)(2,1)}, bf16[2048,256]{1,0:T(8,128)(2,1)}, u32[]{:S(2)}, u32[]{:S(2)}) %collective-permute-start.5) | collective-permute-done | bytes 1048608 | tf_op jit(solution)/shard_map/ppermute | solution.py:14
  120.6 14.7 %hidden_units.1.refs_0_ = bf16[512,1024]{1,0:T(8,128)(2,1)} custom-call(bf16[512,2048]{1,0:T(8,128)(2,1)} %bitcast.10.refs_0_, bf16[2048,256]{1,0:T(8,128)(2,1)} %bitcast.62, bf16[2048,256]{1,0:T(8,128)(2,1)} %bitcast.65, bf16[2048,256]{1,0:T(8,128)(2,1)} %collective-permute-done.1.refs_3_, bf16[2048,256]{1,0:T(8,128)(2,1)} %collective-permute-done.2.refs_4_, ...), custom_call_target="tpu_custom_call" | custom-call | tf_op jit(solution)/shard_map/hidden_units/pallas_call | solution.py:71
  135.3 1.1 slice.69
  136.7 1.1 slice.68
  137.8 1.8 collective-permute-start.9
  139.6 8.9 %collective-permute-done.10.refs_5_ = bf16[128,2048]{1,0:T(8,128)(2,1)} collective-permute-done((bf16[128,2048]{1,0:T(8,128)(2,1)S(1)}, bf16[128,2048]{1,0:T(8,128)(2,1)}, u32[]{:S(2)}, u32[]{:S(2)}) %collective-permute-start.10) | collective-permute-done | bytes 524320 | tf_op jit(solution)/shard_map/ppermute | solution.py:14
  148.5 2.6 %collective-permute-done.9.refs_4_ = bf16[128,2048]{1,0:T(8,128)(2,1)} collective-permute-done((bf16[128,2048]{1,0:T(8,128)(2,1)S(1)}, bf16[128,2048]{1,0:T(8,128)(2,1)}, u32[]{:S(2)}, u32[]{:S(2)}) %collective-permute-start.9) | collective-permute-done | bytes 524320 | tf_op jit(solution)/shard_map/ppermute | solution.py:14
  151.2 5.7 %down_product.1 = bf16[512,2048]{1,0:T(8,128)(2,1)} custom-call(bf16[512,1024]{1,0:T(8,128)(2,1)} %hidden_units.1.refs_0_, bf16[256,2048]{1,0:T(8,128)(2,1)} %bitcast.13.refs_1_, bf16[256,2048]{1,0:T(8,128)(2,1)} %collective-permute-done.7.refs_2_, bf16[256,2048]{1,0:T(8,128)(2,1)} %collective-permute-done.8.refs_3_, ...), custom_call_target="tpu_custom_call" | custom-call | tf_op jit(solution)/shard_map/down_product/pallas_call | solution.py:119
  156.9 10.5 %all-to-all-start.1 = ((bf16[64,8,2048]{2,1,0:T(8,128)(2,1)}), bf16[64,8,2048]{2,1,0:T(8,128)(2,1)}, u32[]{:S(2)}, u32[]{:S(2)}) async-start(bf16[64,8,2048]{2,1,0:T(8,128)(2,1)} %bitcast.59), calls=%async_computation.1 | async-start | bytes 4194304 | tf_op jit(solution)/shard_map/all_to_all | solution.py:24
  167.5 2.0 collective-permute-start.16
  170.2 11.4 %collective-permute-done.14 = bf16[128,2048]{1,0:T(8,128)(2,1)S(1)} collective-permute-done((bf16[128,2048]{1,0:T(8,128)(2,1)}, bf16[128,2048]{1,0:T(8,128)(2,1)S(1)}, u32[]{:S(2)}, u32[]{:S(2)}) %collective-permute-start.14) | collective-permute-done | bytes 524320 | tf_op jit(solution)/shard_map/ppermute | solution.py:14
  182.4 1.5 collective-permute-start.18
  183.9 0.8 copy-done.5
  186.0 1.5 fusion.52
  187.5 3.0 %convolution_convert_fusion.3 = bf16[128,2048]{1,0:T(8,128)(2,1)} fusion(bf16[256,2048]{1,0:T(8,128)(2,1)S(1)} %copy-done.1, f32[128,256]{1,0:T(8,128)S(1)} %fusion.52, bf16[128,2048]{1,0:T(8,128)(2,1)} %copy-done.3, bf16[2048,256]{1,0:T(8,128)(2,1)} %param.26), kind=kOutput, calls=%fused_computation.7 | convolution fusion | flops 268894208 | bytes 3276800 | tf_op jit(solution)/shard_map/dot_general | solution.py:42
  191.4 2.6 %collective-permute-start.13 = (bf16[128,2048]{1,0:T(8,128)(2,1)}, bf16[128,2048]{1,0:T(8,128)(2,1)}, u32[]{:S(2)}, u32[]{:S(2)}) collective-permute-start(bf16[128,2048]{1,0:T(8,128)(2,1)} %convolution_convert_fusion.4), channel_id=1, source_target_pairs={{0,3},{1,0},{2,1},{3,2},{4,7},{5,4},{6,5},{7,6},{8,11},{9,8},{10,9... | collective-permute-start | bytes 1572872 | tf_op jit(solution)/shard_map/ppermute | solution.py:14
  194.0 1.6 collective-permute-done.17
  195.6 1.0 constant_dynamic-update-slice_fusion.1
  197.4 1.5 fusion.54
  199.0 3.0 %convolution_convert_fusion.1 = bf16[128,2048]{1,0:T(8,128)(2,1)} fusion(bf16[256,2048]{1,0:T(8,128)(2,1)S(1)} %copy-done.1, f32[128,256]{1,0:T(8,128)S(1)} %fusion.54, bf16[128,2048]{1,0:T(8,128)(2,1)} %copy-done.4, bf16[2048,256]{1,0:T(8,128)(2,1)} %param.26), kind=kOutput, calls=%fused_computation.4 | convolution fusion | flops 268894208 | bytes 3276800 | tf_op jit(solution)/shard_map/dot_general | solution.py:42
  202.2 14.9 %collective-permute-done.11 = bf16[128,2048]{1,0:T(8,128)(2,1)} collective-permute-done((bf16[128,2048]{1,0:T(8,128)(2,1)}, bf16[128,2048]{1,0:T(8,128)(2,1)}, u32[]{:S(2)}, u32[]{:S(2)}) %collective-permute-start.11) | collective-permute-done | bytes 524320 | tf_op jit(solution)/shard_map/ppermute | solution.py:14
  217.0 2.1 add_convert_fusion.3
  219.1 1.7 fusion.53
  220.9 3.1 %add_convert_fusion.1 = bf16[128,2048]{1,0:T(8,128)(2,1)} fusion(bf16[128,2048]{1,0:T(8,128)(2,1)} %collective-permute-done.19, bf16[256,2048]{1,0:T(8,128)(2,1)S(1)} %copy-done.1, f32[128,256]{1,0:T(8,128)S(1)} %fusion.53, bf16[128,2048]{1,0:T(8,128)(2,1)} %copy-done.5, bf16[2048,256]{1,0:T(8,128)(2,1)} %param.26), kind=kOutput, calls=%fused_computation.31 | convolution fusion | flops 269942784 | bytes 3801088 | tf_op jit(solution)/shard_map/dot_general | solution.py:42
  224.0 3.2 %collective-permute-start.20 = (bf16[128,2048]{1,0:T(8,128)(2,1)}, bf16[128,2048]{1,0:T(8,128)(2,1)}, u32[]{:S(2)}, u32[]{:S(2)}) collective-permute-start(bf16[128,2048]{1,0:T(8,128)(2,1)} %add_convert_fusion.1), channel_id=1, source_target_pairs={{0,3},{1,0},{2,1},{3,2},{4,7},{5,4},{6,5},{7,6},{8,11},{9,8},{10,9... | collective-permute-start | bytes 1572872 | tf_op jit(solution)/shard_map/ppermute | solution.py:14
  227.2 6.3 %collective-permute-done.12 = bf16[128,2048]{1,0:T(8,128)(2,1)} collective-permute-done((bf16[128,2048]{1,0:T(8,128)(2,1)}, bf16[128,2048]{1,0:T(8,128)(2,1)}, u32[]{:S(2)}, u32[]{:S(2)}) %collective-permute-start.12) | collective-permute-done | bytes 524320 | tf_op jit(solution)/shard_map/ppermute | solution.py:14
  233.5 2.4 add_convert_fusion.2
  235.9 2.1 convolution_multiply_fusion.1
  238.1 3.3 %add_convert_fusion = bf16[128,2048]{1,0:T(8,128)(2,1)} fusion(f32[128,2048]{1,0:T(8,128)S(1)} %convolution_multiply_fusion.1, bf16[128,2048]{1,0:T(8,128)(2,1)} %collective-permute-done.20, bf16[128,2048]{1,0:T(8,128)(2,1)} %collective-permute-done.15, bf16[128,2048]{1,0:T(8,128)(2,1)S(1)} %copy-done.6, f32[128]{0:T(128)S(1)} %get-tuple-element.25, ...), kind=kOutput, calls=%fused_computation.30 | convolution fusion | flops 270860288 | bytes 5243904 | tf_op jit(solution)/shard_map/dot_general | solution.py:42
  (59 shorter events, 8.6 us)
Async XLA Ops:
  0.6 77.2 %copy-start = (bf16[512,2048]{1,0:T(8,128)(2,1)S(1)}, bf16[512,2048]{1,0:T(8,128)(2,1)}, u32[]{:S(2)}) copy-start(bf16[512,2048]{1,0:T(8,128)(2,1)} %param.19) | copy-start | bytes 6291460
  5.5 0.8 copy-start.2
  8.4 22.9 %copy-start.1 = (bf16[256,2048]{1,0:T(8,128)(2,1)S(1)}, bf16[256,2048]{1,0:T(8,128)(2,1)}, u32[]{:S(2)}) copy-start(bf16[256,2048]{1,0:T(8,128)(2,1)} %param.27) | copy-start | bytes 3145732
  8.4 74.4 %all-to-all-start = ((bf16[64,8,2048]{2,1,0:T(8,128)(2,1)}), bf16[64,8,2048]{2,1,0:T(8,128)(2,1)}, u32[]{:S(2)}, u32[]{:S(2)}) async-start(bf16[64,8,2048]{2,1,0:T(8,128)(2,1)} %fusion), calls=%async_computation | async-start | bytes 4194304 | tf_op jit(solution)/shard_map/all_to_all | solution.py:24
  20.8 51.7 %collective-permute-start.4 = (bf16[2048,256]{1,0:T(8,128)(2,1)}, bf16[2048,256]{1,0:T(8,128)(2,1)}, u32[]{:S(2)}, u32[]{:S(2)}) collective-permute-start(bf16[2048,256]{1,0:T(8,128)(2,1)} %bitcast.63), channel_id=1, source_target_pairs={{0,3},{1,0},{2,1},{3,2},{4,7},{5,4},{6,5},{7,6},{8,11},{9,8},{10,9... | collective-permute-start | bytes 3145736 | tf_op jit(solution)/shard_map/ppermute | solution.py:14
  23.6 51.0 %collective-permute-start.2 = (bf16[2048,256]{1,0:T(8,128)(2,1)}, bf16[2048,256]{1,0:T(8,128)(2,1)}, u32[]{:S(2)}, u32[]{:S(2)}) collective-permute-start(bf16[2048,256]{1,0:T(8,128)(2,1)} %bitcast.64), channel_id=1, source_target_pairs={{0,1},{1,2},{2,3},{3,0},{4,5},{5,6},{6,7},{7,4},{8,9},{9,10},{10,1... | collective-permute-start | bytes 3145736 | tf_op jit(solution)/shard_map/ppermute | solution.py:14
  23.6 48.9 %collective-permute-start.1 = (bf16[2048,256]{1,0:T(8,128)(2,1)}, bf16[2048,256]{1,0:T(8,128)(2,1)}, u32[]{:S(2)}, u32[]{:S(2)}) collective-permute-start(bf16[2048,256]{1,0:T(8,128)(2,1)} %bitcast.60), channel_id=1, source_target_pairs={{0,1},{1,2},{2,3},{3,0},{4,5},{5,6},{6,7},{7,4},{8,9},{9,10},{10,1... | collective-permute-start | bytes 3145736 | tf_op jit(solution)/shard_map/ppermute | solution.py:14
  24.4 58.4 %collective-permute-start.3 = (bf16[2048,256]{1,0:T(8,128)(2,1)}, bf16[2048,256]{1,0:T(8,128)(2,1)}, u32[]{:S(2)}, u32[]{:S(2)}) collective-permute-start(bf16[2048,256]{1,0:T(8,128)(2,1)} %bitcast.61), channel_id=1, source_target_pairs={{0,3},{1,0},{2,1},{3,2},{4,7},{5,4},{6,5},{7,6},{8,11},{9,8},{10,9... | collective-permute-start | bytes 3145736 | tf_op jit(solution)/shard_map/ppermute | solution.py:14
  27.6 6.7 %copy-start.8 = (bf16[3,512]{1,0:T(4,128)(2,1)S(1)}, bf16[3,512]{1,0:T(4,128)(2,1)}, u32[]{:S(2)}) copy-start(bf16[3,512]{1,0:T(4,128)(2,1)} %param.18) | copy-start | bytes 9220
  27.6 6.7 %collective-permute-start = (bf16[2,2,512]{2,1,0:T(2,128)(2,1)S(1)}, bf16[2,2,512]{2,1,0:T(2,128)(2,1)S(1)}, u32[]{:S(2)}, u32[]{:S(2)}) collective-permute-start(bf16[2,2,512]{2,1,0:T(2,128)(2,1)S(1)} %pad_maximum_fusion), channel_id=1, source_target_pairs={{0,4},{4,8},{8,12},{12,16},{16,20},{20,24},{24,28},{28,32},{32,36}... | collective-permute-start | bytes 12296 | tf_op jit(solution)/shard_map/ppermute | solution.py:20
  34.4 1.5 copy-start.7
  72.5 62.7 %collective-permute-start.8 = (bf16[256,2048]{1,0:T(8,128)(2,1)}, bf16[256,2048]{1,0:T(8,128)(2,1)}, u32[]{:S(2)}, u32[]{:S(2)}) collective-permute-start(bf16[256,2048]{1,0:T(8,128)(2,1)} %bitcast.13.refs_1_), channel_id=1, source_target_pairs={{0,3},{1,0},{2,1},{3,2},{4,7},{5,4},{6,5},{7,6},{8,11},{9,8},{10,9... | collective-permute-start | bytes 3145736 | tf_op jit(solution)/shard_map/ppermute | solution.py:14
  72.5 62.8 %collective-permute-start.7 = (bf16[256,2048]{1,0:T(8,128)(2,1)}, bf16[256,2048]{1,0:T(8,128)(2,1)}, u32[]{:S(2)}, u32[]{:S(2)}) collective-permute-start(bf16[256,2048]{1,0:T(8,128)(2,1)} %bitcast.13.refs_1_), channel_id=1, source_target_pairs={{0,1},{1,2},{2,3},{3,0},{4,5},{5,6},{6,7},{7,4},{8,9},{9,10},{10,1... | collective-permute-start | bytes 3145736 | tf_op jit(solution)/shard_map/ppermute | solution.py:14
  74.6 46.0 %collective-permute-start.5 = (bf16[2048,256]{1,0:T(8,128)(2,1)}, bf16[2048,256]{1,0:T(8,128)(2,1)}, u32[]{:S(2)}, u32[]{:S(2)}) collective-permute-start(bf16[2048,256]{1,0:T(8,128)(2,1)} %collective-permute-done.1.refs_3_), channel_id=1, source_target_pairs={{0,1},{1,2},{2,3},{3,0},{4,5},{5,6},{6,7},{7,4},{8,9},{9,10},{10,1... | collective-permute-start | bytes 3145736 | tf_op jit(solution)/shard_map/ppermute | solution.py:14
  74.6 46.0 %collective-permute-start.6 = (bf16[2048,256]{1,0:T(8,128)(2,1)}, bf16[2048,256]{1,0:T(8,128)(2,1)}, u32[]{:S(2)}, u32[]{:S(2)}) collective-permute-start(bf16[2048,256]{1,0:T(8,128)(2,1)} %collective-permute-done.4.refs_6_), channel_id=1, source_target_pairs={{0,3},{1,0},{2,1},{3,2},{4,7},{5,4},{6,5},{7,6},{8,11},{9,8},{10,9... | collective-permute-start | bytes 3145736 | tf_op jit(solution)/shard_map/ppermute | solution.py:14
  136.4 12.1 %collective-permute-start.10 = (bf16[128,2048]{1,0:T(8,128)(2,1)S(1)}, bf16[128,2048]{1,0:T(8,128)(2,1)}, u32[]{:S(2)}, u32[]{:S(2)}) collective-permute-start(bf16[128,2048]{1,0:T(8,128)(2,1)S(1)} %slice.69), channel_id=1, source_target_pairs={{0,3},{1,0},{2,1},{3,2},{4,7},{5,4},{6,5},{7,6},{8,11},{9,8},{10,9... | collective-permute-start | bytes 1572872 | tf_op jit(solution)/shard_map/ppermute | solution.py:14
  137.8 13.3 %collective-permute-start.9 = (bf16[128,2048]{1,0:T(8,128)(2,1)S(1)}, bf16[128,2048]{1,0:T(8,128)(2,1)}, u32[]{:S(2)}, u32[]{:S(2)}) collective-permute-start(bf16[128,2048]{1,0:T(8,128)(2,1)S(1)} %slice.68), channel_id=1, source_target_pairs={{0,1},{1,2},{2,3},{3,0},{4,5},{5,6},{6,7},{7,4},{8,9},{9,10},{10,1... | collective-permute-start | bytes 1572872 | tf_op jit(solution)/shard_map/ppermute | solution.py:14
  156.9 79.0 %all-to-all-start.1 = ((bf16[64,8,2048]{2,1,0:T(8,128)(2,1)}), bf16[64,8,2048]{2,1,0:T(8,128)(2,1)}, u32[]{:S(2)}, u32[]{:S(2)}) async-start(bf16[64,8,2048]{2,1,0:T(8,128)(2,1)} %bitcast.59), calls=%async_computation.1 | async-start | bytes 4194304 | tf_op jit(solution)/shard_map/all_to_all | solution.py:24
  167.4 14.2 %collective-permute-start.14 = (bf16[128,2048]{1,0:T(8,128)(2,1)}, bf16[128,2048]{1,0:T(8,128)(2,1)S(1)}, u32[]{:S(2)}, u32[]{:S(2)}) collective-permute-start(bf16[128,2048]{1,0:T(8,128)(2,1)} %copy-done.2), channel_id=1, source_target_pairs={{0,3},{1,0},{2,1},{3,2},{4,7},{5,4},{6,5},{7,6},{8,11},{9,8},{10,9... | collective-permute-start | bytes 1572872 | tf_op jit(solution)/shard_map/ppermute | solution.py:14
  167.5 16.4 %collective-permute-start.16 = (bf16[128,2048]{1,0:T(8,128)(2,1)}, bf16[128,2048]{1,0:T(8,128)(2,1)S(1)}, u32[]{:S(2)}, u32[]{:S(2)}) collective-permute-start(bf16[128,2048]{1,0:T(8,128)(2,1)} %copy-done.2), channel_id=1, source_target_pairs={{0,1},{1,2},{2,3},{3,0},{4,5},{5,6},{6,7},{7,4},{8,9},{9,10},{10,1... | collective-permute-start | bytes 1572872 | tf_op jit(solution)/shard_map/ppermute | solution.py:14
  181.6 4.3 %copy-start.3 = (bf16[128,2048]{1,0:T(8,128)(2,1)}, bf16[128,2048]{1,0:T(8,128)(2,1)S(1)}, u32[]{:S(2)}) copy-start(bf16[128,2048]{1,0:T(8,128)(2,1)S(1)} %collective-permute-done.14) | copy-start | bytes 1572868
  182.4 14.2 %collective-permute-start.18 = (bf16[64,2048]{1,0:T(8,128)(2,1)}, bf16[64,2048]{1,0:T(8,128)(2,1)S(1)}, u32[]{:S(2)}, u32[]{:S(2)}) collective-permute-start(bf16[64,2048]{1,0:T(8,128)(2,1)} %slice.71), channel_id=1, source_target_pairs={{0,3},{1,0},{2,1},{3,2},{4,7},{5,4},{6,5},{7,6},{8,11},{9,8},{10,9... | collective-permute-start | bytes 786440 | tf_op jit(solution)/shard_map/ppermute | solution.py:14
  183.9 0.8 copy-start.5
  185.5 10.2 %collective-permute-start.17 = (bf16[64,2048]{1,0:T(8,128)(2,1)}, bf16[64,2048]{1,0:T(8,128)(2,1)}, u32[]{:S(2)}, u32[]{:S(2)}) collective-permute-start(bf16[64,2048]{1,0:T(8,128)(2,1)} %slice.70), channel_id=1, source_target_pairs={{0,1},{1,2},{2,3},{3,0},{4,5},{5,6},{6,7},{7,4},{8,9},{9,10},{10,1... | collective-permute-start | bytes 786440 | tf_op jit(solution)/shard_map/ppermute | solution.py:14
  190.5 47.6 %collective-permute-start.15 = (bf16[128,2048]{1,0:T(8,128)(2,1)}, bf16[128,2048]{1,0:T(8,128)(2,1)}, u32[]{:S(2)}, u32[]{:S(2)}) collective-permute-start(bf16[128,2048]{1,0:T(8,128)(2,1)} %convolution_convert_fusion.3), channel_id=1, source_target_pairs={{0,1},{1,2},{2,3},{3,0},{4,5},{5,6},{6,7},{7,4},{8,9},{9,10},{10,1... | collective-permute-start | bytes 1572872 | tf_op jit(solution)/shard_map/ppermute | solution.py:14
  190.8 26.2 %collective-permute-start.11 = (bf16[128,2048]{1,0:T(8,128)(2,1)}, bf16[128,2048]{1,0:T(8,128)(2,1)}, u32[]{:S(2)}, u32[]{:S(2)}) collective-permute-start(bf16[128,2048]{1,0:T(8,128)(2,1)} %convolution_convert_fusion.6), channel_id=1, source_target_pairs={{0,1},{1,2},{2,3},{3,0},{4,5},{5,6},{6,7},{7,4},{8,9},{9,10},{10,1... | collective-permute-start | bytes 1572872 | tf_op jit(solution)/shard_map/ppermute | solution.py:14
  191.4 35.8 %collective-permute-start.13 = (bf16[128,2048]{1,0:T(8,128)(2,1)}, bf16[128,2048]{1,0:T(8,128)(2,1)}, u32[]{:S(2)}, u32[]{:S(2)}) collective-permute-start(bf16[128,2048]{1,0:T(8,128)(2,1)} %convolution_convert_fusion.4), channel_id=1, source_target_pairs={{0,3},{1,0},{2,1},{3,2},{4,7},{5,4},{6,5},{7,6},{8,11},{9,8},{10,9... | collective-permute-start | bytes 1572872 | tf_op jit(solution)/shard_map/ppermute | solution.py:14
  196.6 0.8 copy-start.4
  202.0 18.9 %collective-permute-start.19 = (bf16[128,2048]{1,0:T(8,128)(2,1)}, bf16[128,2048]{1,0:T(8,128)(2,1)}, u32[]{:S(2)}, u32[]{:S(2)}) collective-permute-start(bf16[128,2048]{1,0:T(8,128)(2,1)} %convolution_convert_fusion.1), channel_id=1, source_target_pairs={{0,3},{1,0},{2,1},{3,2},{4,7},{5,4},{6,5},{7,6},{8,11},{9,8},{10,9... | collective-permute-start | bytes 1572872 | tf_op jit(solution)/shard_map/ppermute | solution.py:14
  219.1 14.4 %collective-permute-start.12 = (bf16[128,2048]{1,0:T(8,128)(2,1)}, bf16[128,2048]{1,0:T(8,128)(2,1)}, u32[]{:S(2)}, u32[]{:S(2)}) collective-permute-start(bf16[128,2048]{1,0:T(8,128)(2,1)} %add_convert_fusion.3), channel_id=1, source_target_pairs={{0,1},{1,2},{2,3},{3,0},{4,5},{5,6},{6,7},{7,4},{8,9},{9,10},{10,1... | collective-permute-start | bytes 1572872 | tf_op jit(solution)/shard_map/ppermute | solution.py:14
  224.0 14.1 %collective-permute-start.20 = (bf16[128,2048]{1,0:T(8,128)(2,1)}, bf16[128,2048]{1,0:T(8,128)(2,1)}, u32[]{:S(2)}, u32[]{:S(2)}) collective-permute-start(bf16[128,2048]{1,0:T(8,128)(2,1)} %add_convert_fusion.1), channel_id=1, source_target_pairs={{0,3},{1,0},{2,1},{3,2},{4,7},{5,4},{6,5},{7,6},{8,11},{9,8},{10,9... | collective-permute-start | bytes 1572872 | tf_op jit(solution)/shard_map/ppermute | solution.py:14
  235.9 2.2 copy-start.6

commit v2 on v1

v2 whole, which is shorter than its diff:
```python
from functools import partial

import jax
import jax.numpy as jnp
from jax import lax
from jax.experimental import pallas as pl
from jax.experimental.pallas import tpu as pltpu
from jax.sharding import PartitionSpec as P


epsilon = 1e-06


def swapped(array, axis, partner):
    return lax.ppermute(
        array, axis, [(i, partner(i)) for i in range(lax.axis_size(axis))]
    )


def shifted(block, axis, distance):
    devices = range(lax.axis_size(axis))
    route = [(i - distance, i) for i in devices if i - distance in devices]
    return lax.ppermute(block, axis, route)


def moved(block, target):
    tp_count, cores = lax.axis_size("tp"), 2
    route = []
    for index in range(lax.axis_size("ep") * tp_count):
        chip, core, place = index // tp_count // cores, index // tp_count % cores, index % tp_count
        goal = target(core, place)
        if goal is not None:
            route.append((index, (chip * cores + goal[0]) * tp_count + goal[1]))
    return lax.ppermute(block, ("ep", "tp"), route)


def across(block):
    return swapped(block, "tp", lambda place: 3 - place)


def beside(block):
    return swapped(block, "tp", lambda place: place ^ 1)


def is_ours(core, place):
    return (core == 0) == (place < 2)


def to_host(core, place):
    return (core, place ^ 1) if is_ours(core, place) else (1 - core, 3 - place)


def to_pair(core, place):
    return None if is_ours(core, place) else (core, place ^ 1)


def to_core(core, place):
    return 1 - core, place


def exchanged(blocks):
    tp_count, cores = lax.axis_size("tp"), 2
    chips = lax.axis_size("ep") // cores
    groups = []
    for core in range(cores):
        for even, odd in ((0, 3), (1, 2)):
            groups.append(
                [
                    (chip * cores + core) * tp_count + place
                    for chip in range(chips)
                    for place in (even, odd)
                ]
            )
    return lax.all_to_all(blocks, ("ep", "tp"), 0, 0, axis_index_groups=groups, tiled=True)


def times(first, second):
    return first.astype(jnp.float32) * second.astype(jnp.float32)


def both(first, second):
    return first.astype(jnp.float32) + second.astype(jnp.float32)


def after(value, *others):
    return lax.optimization_barrier((value, *others))[0]


def dot(left, right):
    return jnp.dot(left, right, preferred_element_type=jnp.float32)


def swiglu(inputs, gate_w, up_w):
    return (jax.nn.silu(dot(inputs, gate_w)) * dot(inputs, up_w)).astype(jnp.bfloat16)


def expert_kernel(*refs, count):
    x_hbm, ups, downs, out = refs[0], refs[1 : 1 + 2 * count], refs[1 + 2 * count : -8], refs[-8]
    x, held, down, hidden, sums, sems, out_sems = refs[-7:]
    units = downs[0].shape[0]
    copies = [pltpu.make_async_copy(x_hbm, x, sems.at[0])]
    for i, block in enumerate(ups):
        copies.append(pltpu.make_async_copy(block, held.at[i], sems.at[1 + i]))
    for i, block in enumerate(downs):
        place = down.at[pl.ds(i * units, units)]
        copies.append(pltpu.make_async_copy(block, place, sems.at[1 + 2 * count + i]))
    for copy in copies:
        copy.start()
    copies[0].wait()
    for i in range(count):
        copies[1 + 2 * i].wait()
        copies[2 + 2 * i].wait()
        gate_term, upward = dot(x[...], held[2 * i]), dot(x[...], held[2 * i + 1])
        hidden[:, i * units : (i + 1) * units] = (jax.nn.silu(gate_term) * upward).astype(x.dtype)
    for i in range(count):
        copies[1 + 2 * count + i].wait()
    tiles, _, width = sums.shape
    stores = []
    for t in range(tiles):
        sums[t] = dot(hidden[...], down[:, t * width : (t + 1) * width]).astype(x.dtype)
        place = out.at[:, pl.ds(t * width, width)]
        stores.append(pltpu.make_async_copy(sums.at[t], place, out_sems.at[t]))
        stores[-1].start()
    for store in stores:
        store.wait()


def expert(rows, ups, downs, tiles=4):
    count, units, width = len(downs), *downs[0].shape
    dtype = rows.dtype
    anywhere = pl.BlockSpec(memory_space=pl.ANY)
    return pl.pallas_call(
        partial(expert_kernel, count=count),
        out_shape=jax.ShapeDtypeStruct(rows.shape, dtype),
        in_specs=[anywhere] * (1 + 3 * count),
        out_specs=anywhere,
        scratch_shapes=[
            pltpu.VMEM(rows.shape, dtype),
            pltpu.VMEM((2 * count, *ups[0].shape), dtype),
            pltpu.VMEM((count * units, width), dtype),
            pltpu.VMEM((rows.shape[0], count * units), dtype),
            pltpu.VMEM((tiles, rows.shape[0], width // tiles), dtype),
            pltpu.SemaphoreType.DMA((1 + 3 * count,)),
            pltpu.SemaphoreType.DMA((tiles,)),
        ],
        name="expert",
    )(rows, *ups, *downs)


def dispatch_kernel(x_ref, gain_ref, routes_ref, normed_ref, out_ref, slots_ref, *, experts):
    tokens = x_ref.shape[0]
    capacity = out_ref.shape[0] // experts
    values = x_ref[...].astype(jnp.float32)
    square = jnp.mean(values * values, axis=-1, keepdims=True)
    scaled = values * lax.rsqrt(square + epsilon) * gain_ref[...].astype(jnp.float32)
    normed = scaled.astype(jnp.bfloat16)
    normed_ref[...] = normed
    mine = pl.ds(pl.multiple_of(lax.axis_index("tp") * tokens, tokens), tokens)
    choices = [routes_ref[k : k + 1, mine] for k in range(routes_ref.shape[0])]
    expert = lax.broadcasted_iota(jnp.int32, (experts, tokens), 0)
    hits = [jnp.where(expert == choice, 1.0, 0.0) for choice in choices]
    rows = lax.broadcasted_iota(jnp.int32, (tokens, tokens), 0)
    cols = lax.broadcasted_iota(jnp.int32, (tokens, tokens), 1)
    before = jnp.where(rows < cols, 1.0, 0.0).astype(jnp.bfloat16)
    earlier = dot((hits[0] + hits[1]).astype(jnp.bfloat16), before)
    slot_ids = lax.broadcasted_iota(jnp.int32, (out_ref.shape[0], tokens), 0)
    chosen = None
    for k, choice in enumerate(choices):
        rank = jnp.sum(earlier * hits[k], axis=0, keepdims=True).astype(jnp.int32)
        slots = choice * capacity + rank
        slots_ref[k : k + 1, :] = slots
        match = slot_ids == slots
        chosen = match if chosen is None else chosen | match
    chosen = jnp.where(chosen, 1.0, 0.0).astype(jnp.bfloat16)
    out_ref[...] = dot(chosen, normed).astype(jnp.bfloat16)


def dispatched(moe_input, norm_gain, routes, experts, capacity):
    tokens, width = moe_input.shape
    in_vmem = pl.BlockSpec(memory_space=pltpu.VMEM)
    return pl.pallas_call(
        partial(dispatch_kernel, experts=experts),
        out_shape=(
            jax.ShapeDtypeStruct((tokens, width), jnp.bfloat16),
            jax.ShapeDtypeStruct((experts * capacity, width), jnp.bfloat16),
            jax.ShapeDtypeStruct((routes.shape[1], tokens), jnp.int32),
        ),
        in_specs=[in_vmem] * 3,
        out_specs=[in_vmem] * 3,
        name="dispatched",
    )(moe_input, norm_gain.reshape(1, width), routes.T)


def per_device(
    outer_gate,
    inner_gate,
    conv_values,
    conv_taps,
    out_weight,
    moe_input,
    norm_gain,
    gate_proj,
    up_proj,
    down_proj,
    shared_gate,
    shared_up,
    shared_down,
    routes,
    route_weight,
):
    tp_count = lax.axis_size("tp")
    ep_count = lax.axis_size("ep")
    my_slot = lax.axis_index("tp")
    group_len = inner_gate.shape[0]
    mix_rows = group_len // tp_count
    model_width = moe_input.shape[1]
    own_rows = moe_input.shape[0]
    top_count = routes.shape[1]
    capacity = 2 * own_rows * top_count // ep_count
    slot_rows = ep_count * capacity
    reach_rows = conv_taps.shape[0] - 1

    ours = (lax.axis_index("ep") % 2 == 0) == (my_slot < 2)
    weights = {"gate": gate_proj[0], "up": up_proj[0], "down": down_proj[0]}
    first = {name: moved(block, to_host) for name, block in weights.items()}
    second, third, fourth = {}, {}, {}

    def bring(name):
        second[name] = moved(first[name], to_pair)

    def spread(name, *earlier):
        third[name] = moved(first[name], to_core)
        second[name] = jnp.where(ours, weights[name], after(second[name], *earlier))
        fourth[name] = moved(second[name], to_core)

    tail = slice(group_len - reach_rows, group_len)
    before = shifted(times(inner_gate[tail], conv_values[tail]), "ep", 1)

    normed, outgoing, slots = dispatched(moe_input, norm_gain, routes, ep_count, capacity)
    slots = slots.T
    own_weights = lax.dynamic_slice_in_dim(route_weight, my_slot * own_rows, own_rows, 0)
    landed = exchanged(outgoing.reshape(ep_count, capacity, model_width))
    landed = landed.reshape(slot_rows, model_width)

    for name in weights:
        bring(name)
    product = jnp.concatenate((before, times(inner_gate, conv_values)), axis=0)
    tap_values = conv_taps.astype(jnp.float32)
    convolved = tap_values[0] * product[0:group_len]
    for offset in range(1, reach_rows + 1):
        convolved = convolved + tap_values[offset] * product[offset : offset + group_len]
    gate_rows = (outer_gate.astype(jnp.float32) * convolved).astype(jnp.bfloat16)
    mix = {}
    places = {"own": my_slot, "across": 3 - my_slot, "beside": my_slot ^ 1, "far": 3 - my_slot ^ 1}
    for key, place in places.items():
        rows = lax.dynamic_slice_in_dim(gate_rows, place * mix_rows, mix_rows, 0)
        mix[key] = dot(rows, out_weight).astype(jnp.bfloat16)

    def shared_part(rows):
        return dot(swiglu(rows, shared_gate, shared_up), shared_down).astype(jnp.bfloat16)

    normed_across = across(normed)
    normed_beside = beside(normed)
    shared = {"own": shared_part(normed)}
    early = (*mix.values(), *shared.values())
    spread("gate", *early)
    spread("up", second["gate"])
    spread("down", second["up"])

    landed = after(landed, *early)
    blocks = (first, third, second, fourth)
    ups = [w[name] for w in blocks for name in ("gate", "up")]
    total = expert(landed, ups, [w["down"] for w in blocks])
    returned = exchanged(total.reshape(ep_count, capacity, model_width))
    returned = returned.reshape(slot_rows, model_width)

    normed_far = beside(normed_across)

    got_own = across(mix["across"])
    got_beside = after(across(mix["far"]), total)
    got_rest = beside(both(mix["beside"], got_beside).astype(jnp.bfloat16))
    mixer_out = both(mix["own"], got_own) + got_rest.astype(jnp.float32)

    shared["far"] = shared_part(after(normed_far, total))
    shared["beside"] = shared_part(after(normed_beside, total))
    shared["across"] = shared_part(after(normed_across, total))
    got_across = beside(shared["far"])
    got_own = beside(shared["beside"])
    got_rest = across(both(shared["across"], got_across).astype(jnp.bfloat16))
    shared_total = both(shared["own"], got_own) + got_rest.astype(jnp.float32)

    slot_ids = lax.broadcasted_iota(jnp.int32, (own_rows, slot_rows), 1)
    routed = shared_total
    for choice in range(top_count):
        picks = (slot_ids == slots[:, choice][:, None]).astype(jnp.bfloat16)
        routed = routed + dot(picks, returned) * own_weights[:, choice][:, None]
    return (mixer_out.astype(jnp.bfloat16), routed.astype(jnp.bfloat16))


def solution(mesh):
    return jax.shard_map(
        per_device,
        mesh=mesh,
        in_specs=(
            P("ep", "tp"),
            P("ep", "tp"),
            P("ep", "tp"),
            P(None, "tp"),
            P("tp", None),
            P(("ep", "tp"), None),
            P(),
            P("ep", None, "tp"),
            P("ep", None, "tp"),
            P("ep", "tp", None),
            P(None, "tp"),
            P(None, "tp"),
            P("tp", None),
            P("ep", None),
            P("ep", None),
        ),
        out_specs=(P(("ep", "tp"), None), P(("ep", "tp"), None)),
        check_vma=False,
    )
```

time: 243 us -> 193 us (0.79)
  waiting for transfers between devices: 120 us -> 53.7 us
  starting transfers between devices: 49.4 us -> 76.7 us
  Pallas kernels: 20.4 us -> 13.8 us
  local copies, waits for them, and re-layouts: 9.33 us -> 3.63 us
  other arithmetic: 10.3 us -> 14.2 us
    ppermute x20 -> x21, waiting for transfers between devices: 120 us -> 52.3 us  [the longest x9 49.6 us: swapped(): lax.ppermute(array, axis, [(i, partner(i)) for i in range(lax.axis_size(a...]
    ppermute x20 -> x21, starting transfers between devices: 24.6 us -> 44.4 us  [the longest x12 34.3 us: moved(): return lax.ppermute(block, ('ep', 'tp'), route)]
    all_to_all x2, starting transfers between devices: 22.9 us -> 30.5 us  [exchanged(): lax.all_to_all(blocks, ('ep', 'tp'), 0, 0, axis_index_groups=groups, tile...]
    pallas_call x2, Pallas kernels: 20.4 us -> 13.8 us  [the longest x1 10.5 us: expert(): pl.pallas_call(partial(expert_kernel, count=count), out_shape=jax.ShapeDt...]
    slice x4 -> x0, local copies, waits for them, and re-layouts: 3.65 us -> none  [the longest x1 1.08 us: per_device(): down_p1 = turn(down_r[half_units:], 'tp', -1)]
    select_n x0 -> x3, other arithmetic: none -> 3.26 us  [spread(): second[name] = jnp.where(ours, weights[name], after(second[name], *earlier))]
    convert_element_type x1, other arithmetic: 0.4 us -> 2.92 us  [per_device(): (outer_gate.astype(jnp.float32) * convolved).astype(jnp.bfloat16)]
    dot_general x16 -> x14, matrix products: 31.2 us -> 28.8 us  [dot(): return jnp.dot(left, right, preferred_element_type=jnp.float32)]
  transfers between devices with their start and end apart: 23 -> 24, of which waited for: 8 -> 8; matrix products, arithmetic and copies ran while one was open for 15% -> 20% of each run, Pallas kernels for 6% -> 2%
where the time goes in v2:
time: 193 us; the launch traced here: 192 us
  starting transfers between devices  76.7 us (40%)
  waiting for transfers between devices  53.7 us (28%)
  matrix products  28.8 us (15%)
  other arithmetic  14.2 us (7%)
  Pallas kernels  13.8 us (7%)
  local copies, waits for them, and re-layouts  3.63 us (2%)
    ppermute x9, waiting for transfers between devices, swapped(): lax.ppermute(array, axis, [(i, partner(i)) for i in range(lax.axis_size(a...  49.6 us
    ppermute x12, starting transfers between devices, moved(): return lax.ppermute(block, ('ep', 'tp'), route)  34.3 us
    all_to_all x2, starting transfers between devices, exchanged(): lax.all_to_all(blocks, ('ep', 'tp'), 0, 0, axis_index_groups=groups, tile...  30.5 us
    dot_general x14, matrix products, dot(): return jnp.dot(left, right, preferred_element_type=jnp.float32)  28.8 us
    pallas_call x1, Pallas kernels, expert(): pl.pallas_call(partial(expert_kernel, count=count), out_shape=jax.ShapeDt...  10.5 us
    ppermute x9, starting transfers between devices, swapped(): lax.ppermute(array, axis, [(i, partner(i)) for i in range(lax.axis_size(a...  10.1 us
  transfers between devices with their start and end apart: 24, of which 8 were waited for; matrix products, arithmetic and copies ran while one was open for 20% of the time, Pallas kernels for 2%

profile of v2, /device:TPU:8, one launch (start us, length us, event | category | flops | bytes accessed | tf_op | source)
XLA Modules:
  0.0 191.7 jit_solution(14184181912191615954)
XLA Ops:
  0.6 0.9 convert_multiply_fusion.1
  1.5 1.9 collective-permute-start
  3.4 1.6 collective-permute-start.3
  5.5 1.5 collective-permute-start.11
  7.0 1.3 reshape.19.gain_ref
  8.3 3.3 %dispatched.1 = (bf16[128,2048]{1,0:T(8,128)(2,1)}, bf16[512,2048]{1,0:T(8,128)(2,1)}, s32[2,128]{1,0:T(2,128)}) custom-call(bf16[128,2048]{1,0:T(8,128)(2,1)} %x_ref.1, bf16[1,2048]{1,0:T(2,128)(2,1)} %reshape.19.gain_ref, s32[2,512]{1,0:T(2,128)} %bitcast.59), custom_call_target="tpu_custom_call" | custom-call | tf_op jit(solution)/shard_map/dispatched/pallas_call | solution.py:181
  11.7 15.4 %all-to-all-start = ((bf16[64,8,2048]{2,1,0:T(8,128)(2,1)}), bf16[64,8,2048]{2,1,0:T(8,128)(2,1)}, u32[]{:S(2)}, u32[]{:S(2)}) async-start(bf16[64,8,2048]{2,1,0:T(8,128)(2,1)} %bitcast.52), calls=%async_computation | async-start | bytes 4194304 | tf_op jit(solution)/shard_map/all_to_all | solution.py:74
  27.1 2.6 %convert_multiply_fusion = f32[512,512]{1,0:T(8,128)} fusion(bf16[512,512]{1,0:T(8,128)(2,1)} %param.17, bf16[512,512]{1,0:T(8,128)(2,1)} %param.16), kind=kLoop, calls=%fused_computation.31 | loop fusion | flops 786432 | bytes 2097152 | tf_op jit(solution)/shard_map/mul | solution.py:78
  29.7 1.4 fusion.44
  31.0 3.0 %convolution_convert_fusion.3 = bf16[128,2048]{1,0:T(8,128)(2,1)} fusion(bf16[256,2048]{1,0:T(8,128)(2,1)S(1)} %copy-done.1, bf16[128,2048]{1,0:T(8,128)(2,1)} %get-tuple-element.14, bf16[2048,256]{1,0:T(8,128)(2,1)} %param.26, f32[128,256]{1,0:T(8,128)S(1)} %fusion.44), kind=kOutput, calls=%fused_computation.9 | convolution fusion | flops 268894208 | bytes 3276800 | tf_op jit(solution)/shard_map/dot_general | solution.py:90
  34.1 2.9 %fusion.12 = bf16[512,512]{1,0:T(8,128)(2,1)S(1)} fusion(f32[2,512]{1,0:T(2,128)S(1)} %collective-permute-done, f32[512,512]{1,0:T(8,128)} %convert_multiply_fusion, bf16[512,512]{1,0:T(8,128)(2,1)} %param.15, f32[512]{0:T(512)S(1)} %bitcast.58, f32[512]{0:T(512)S(1)} %bitcast.57, f32[512]{0:T(512)S(1)} %bitcast.56), kind=kLoop, calls=%fused_computation.25 | loop fusion | flops 2621440 | bytes 2107392 | tf_op jit(solution)/shard_map/convert_element_type | solution.py:252
  37.7 1.3 convolution_convert_fusion.6
  39.0 1.2 convolution_convert_fusion.4
  40.2 0.8 collective-permute-start.8
  41.1 1.2 convolution_convert_fusion.7
  42.4 1.2 convolution_convert_fusion.5
  43.6 0.8 collective-permute-start.13
  44.5 15.0 %collective-permute-start.12 = (bf16[256,2048]{1,0:T(8,128)(2,1)}, bf16[256,2048]{1,0:T(8,128)(2,1)}, u32[]{:S(2)}, u32[]{:S(2)}) collective-permute-start(bf16[256,2048]{1,0:T(8,128)(2,1)} %collective-permute-done.11.refs_9_), channel_id=1, source_target_pairs={{0,4},{1,5},{2,6},{3,7},{4,0},{5,1},{6,2},{7,3},{8,12},{9,13},{10,... | collective-permute-start | bytes 3145736 | tf_op jit(solution)/shard_map/ppermute | solution.py:34
  60.0 1.1 broadcast_select_fusion.2.refs_5_
  61.1 1.1 broadcast_select_fusion.1.refs_6_
  62.1 2.6 %collective-permute-start.10 = (bf16[2048,256]{1,0:T(8,128)(2,1)}, bf16[2048,256]{1,0:T(8,128)(2,1)}, u32[]{:S(2)}, u32[]{:S(2)}) collective-permute-start(bf16[2048,256]{1,0:T(8,128)(2,1)} %broadcast_select_fusion.1.refs_6_), channel_id=1, source_target_pairs={{0,4},{1,5},{2,6},{3,7},{4,0},{5,1},{6,2},{7,3},{8,12},{9,13},{10,... | collective-permute-start | bytes 3145736 | tf_op jit(solution)/shard_map/ppermute | solution.py:34
  64.8 1.1 broadcast_select_fusion.refs_11_
  65.9 10.2 %collective-permute-start.14 = (bf16[256,2048]{1,0:T(8,128)(2,1)}, bf16[256,2048]{1,0:T(8,128)(2,1)}, u32[]{:S(2)}, u32[]{:S(2)}) collective-permute-start(bf16[256,2048]{1,0:T(8,128)(2,1)} %broadcast_select_fusion.refs_11_), channel_id=1, source_target_pairs={{0,4},{1,5},{2,6},{3,7},{4,0},{5,1},{6,2},{7,3},{8,12},{9,13},{10,... | collective-permute-start | bytes 3145736 | tf_op jit(solution)/shard_map/ppermute | solution.py:34
  76.0 1.4 all-to-all-done
  77.5 1.2 collective-permute-done.14.refs_12_
  78.6 1.5 collective-permute-done.9.refs_7_
  80.1 10.5 %expert.1 = bf16[512,2048]{1,0:T(8,128)(2,1)} custom-call(bf16[512,2048]{1,0:T(8,128)(2,1)} %bitcast.5.refs_0_, bf16[2048,256]{1,0:T(8,128)(2,1)} %collective-permute-done.3.refs_1_, bf16[2048,256]{1,0:T(8,128)(2,1)} %collective-permute-done.4.refs_2_, bf16[2048,256]{1,0:T(8,128)(2,1)} %collective-permute-done.5.refs_3_, ...), custom_call_target="tpu_custom_call" | custom-call | tf_op jit(solution)/shard_map/expert/pallas_call | solution.py:132
  90.7 15.1 %all-to-all-start.1 = ((bf16[64,8,2048]{2,1,0:T(8,128)(2,1)}), bf16[64,8,2048]{2,1,0:T(8,128)(2,1)}, u32[]{:S(2)}, u32[]{:S(2)}) async-start(bf16[64,8,2048]{2,1,0:T(8,128)(2,1)} %bitcast.51), calls=%async_computation.1 | async-start | bytes 4194304 | tf_op jit(solution)/shard_map/all_to_all | solution.py:74
  105.8 2.8 %collective-permute-start.18 = (bf16[128,2048]{1,0:T(8,128)(2,1)}, bf16[128,2048]{1,0:T(8,128)(2,1)}, u32[]{:S(2)}, u32[]{:S(2)}) collective-permute-start(bf16[128,2048]{1,0:T(8,128)(2,1)} %get-tuple-element.14), channel_id=1, source_target_pairs={{0,3},{1,2},{2,1},{3,0},{4,7},{5,6},{6,5},{7,4},{8,11},{9,10},{10,... | collective-permute-start | bytes 1572872 | tf_op jit(solution)/shard_map/ppermute | solution.py:15
  109.8 2.7 %collective-permute-start.1 = (bf16[128,2048]{1,0:T(8,128)(2,1)}, bf16[128,2048]{1,0:T(8,128)(2,1)}, u32[]{:S(2)}, u32[]{:S(2)}) collective-permute-start(bf16[128,2048]{1,0:T(8,128)(2,1)} %convolution_convert_fusion.6), channel_id=1, source_target_pairs={{0,3},{1,2},{2,1},{3,0},{4,7},{5,6},{6,5},{7,4},{8,11},{9,10},{10,... | collective-permute-start | bytes 1572872 | tf_op jit(solution)/shard_map/ppermute | solution.py:15
  112.4 21.7 %collective-permute-done.18 = bf16[128,2048]{1,0:T(8,128)(2,1)} collective-permute-done((bf16[128,2048]{1,0:T(8,128)(2,1)}, bf16[128,2048]{1,0:T(8,128)(2,1)}, u32[]{:S(2)}, u32[]{:S(2)}) %collective-permute-start.18) | collective-permute-done | bytes 524320 | tf_op jit(solution)/shard_map/ppermute | solution.py:15
  134.2 0.8 copy-done.3
  135.0 1.5 fusion.45
  136.6 3.0 %convolution_convert_fusion.2 = bf16[128,2048]{1,0:T(8,128)(2,1)} fusion(bf16[256,2048]{1,0:T(8,128)(2,1)S(1)} %copy-done.1, f32[128,256]{1,0:T(8,128)S(1)} %fusion.45, bf16[128,2048]{1,0:T(8,128)(2,1)} %copy-done.3, bf16[2048,256]{1,0:T(8,128)(2,1)} %param.26), kind=kOutput, calls=%fused_computation.8 | convolution fusion | flops 268894208 | bytes 3276800 | tf_op jit(solution)/shard_map/dot_general | solution.py:90
  139.5 2.0 %collective-permute-start.17 = (bf16[128,2048]{1,0:T(8,128)(2,1)}, bf16[128,2048]{1,0:T(8,128)(2,1)}, u32[]{:S(2)}, u32[]{:S(2)}) collective-permute-start(bf16[128,2048]{1,0:T(8,128)(2,1)} %convolution_convert_fusion.2), channel_id=1, source_target_pairs={{0,1},{1,0},{2,3},{3,2},{4,5},{5,4},{6,7},{7,6},{8,9},{9,8},{10,11... | collective-permute-start | bytes 1572872 | tf_op jit(solution)/shard_map/ppermute | solution.py:15
  141.5 7.8 %collective-permute-done.19 = bf16[128,2048]{1,0:T(8,128)(2,1)} collective-permute-done((bf16[128,2048]{1,0:T(8,128)(2,1)}, bf16[128,2048]{1,0:T(8,128)(2,1)}, u32[]{:S(2)}, u32[]{:S(2)}) %collective-permute-start.19) | collective-permute-done | bytes 524320 | tf_op jit(solution)/shard_map/ppermute | solution.py:15
  149.3 1.7 fusion.47
  151.0 3.0 %convolution_convert_fusion = bf16[128,2048]{1,0:T(8,128)(2,1)} fusion(bf16[256,2048]{1,0:T(8,128)(2,1)S(1)} %copy-done.1, f32[128,256]{1,0:T(8,128)S(1)} %fusion.47, bf16[128,2048]{1,0:T(8,128)(2,1)} %collective-permute-done.19, bf16[2048,256]{1,0:T(8,128)(2,1)} %param.26), kind=kOutput, calls=%fused_computation.5 | convolution fusion | flops 268894208 | bytes 3276800 | tf_op jit(solution)/shard_map/dot_general | solution.py:90
  154.0 2.1 %add_convert_fusion.2 = bf16[128,2048]{1,0:T(8,128)(2,1)} fusion(bf16[128,2048]{1,0:T(8,128)(2,1)} %collective-permute-done.2, bf16[128,2048]{1,0:T(8,128)(2,1)} %convolution_convert_fusion.5), kind=kLoop, calls=%fused_computation.30 | loop fusion | flops 1048576 | bytes 1572864 | tf_op jit(solution)/shard_map/convert_element_type | solution.py:281
  156.1 2.0 %collective-permute-start.15 = (bf16[128,2048]{1,0:T(8,128)(2,1)}, bf16[128,2048]{1,0:T(8,128)(2,1)}, u32[]{:S(2)}, u32[]{:S(2)}) collective-permute-start(bf16[128,2048]{1,0:T(8,128)(2,1)} %add_convert_fusion.2), channel_id=1, source_target_pairs={{0,1},{1,0},{2,3},{3,2},{4,5},{5,4},{6,7},{7,6},{8,9},{9,8},{10,11... | collective-permute-start | bytes 1572872 | tf_op jit(solution)/shard_map/ppermute | solution.py:15
  158.2 1.7 fusion.46
  159.9 11.9 %collective-permute-done.20 = bf16[128,2048]{1,0:T(8,128)(2,1)} collective-permute-done((bf16[128,2048]{1,0:T(8,128)(2,1)}, bf16[128,2048]{1,0:T(8,128)(2,1)}, u32[]{:S(2)}, u32[]{:S(2)}) %collective-permute-start.20) | collective-permute-done | bytes 524320 | tf_op jit(solution)/shard_map/ppermute | solution.py:15
  171.8 3.1 %add_convert_fusion = bf16[128,2048]{1,0:T(8,128)(2,1)} fusion(bf16[128,2048]{1,0:T(8,128)(2,1)} %collective-permute-done.20, bf16[256,2048]{1,0:T(8,128)(2,1)S(1)} %copy-done.1, f32[128,256]{1,0:T(8,128)S(1)} %fusion.46, bf16[128,2048]{1,0:T(8,128)(2,1)} %collective-permute-done.18, bf16[2048,256]{1,0:T(8,128)(2,1)} %param.26), kind=kOutput, calls=%fused_computation.28 | convolution fusion | flops 269942784 | bytes 3801088 | tf_op jit(solution)/shard_map/dot_general | solution.py:90
  174.9 4.4 %collective-permute-done.15 = bf16[128,2048]{1,0:T(8,128)(2,1)} collective-permute-done((bf16[128,2048]{1,0:T(8,128)(2,1)}, bf16[128,2048]{1,0:T(8,128)(2,1)}, u32[]{:S(2)}, u32[]{:S(2)}) %collective-permute-start.15) | collective-permute-done | bytes 524320 | tf_op jit(solution)/shard_map/ppermute | solution.py:15
  179.3 2.4 %add_convert_fusion.1 = bf16[128,2048]{1,0:T(8,128)(2,1)} fusion(bf16[128,2048]{1,0:T(8,128)(2,1)} %collective-permute-done.15, bf16[128,2048]{1,0:T(8,128)(2,1)} %collective-permute-done.1, bf16[128,2048]{1,0:T(8,128)(2,1)} %convolution_convert_fusion.7), kind=kLoop, calls=%fused_computation.29 | loop fusion | flops 1572864 | bytes 2097152 | tf_op jit(solution)/shard_map/convert_element_type | solution.py:297
  181.6 3.8 %collective-permute-done.21 = bf16[128,2048]{1,0:T(8,128)(2,1)S(1)} collective-permute-done((bf16[128,2048]{1,0:T(8,128)(2,1)}, bf16[128,2048]{1,0:T(8,128)(2,1)S(1)}, u32[]{:S(2)}, u32[]{:S(2)}) %collective-permute-start.21) | collective-permute-done | bytes 524320 | tf_op jit(solution)/shard_map/ppermute | solution.py:15
  186.3 2.6 %fusion.1 = f32[128,2048]{1,0:T(8,128)S(1)} fusion(bf16[64,8,2048]{2,1,0:T(8,128)(2,1)} %all-to-all-done.1, bf16[128,2048]{1,0:T(8,128)(2,1)} %copy-done.7, bf16[128,2048]{1,0:T(8,128)(2,1)} %collective-permute-done.17, bf16[128,2048]{1,0:T(8,128)(2,1)} %convolution_convert_fusion.3, f32[128]{0:T(128)S(1)} %get-tuple-element.30, s32[128]{0:T(128)S(1)} %get-tuple-element.28), kind=kOutput, calls=%fused_computation.3 | convolution fusion | flops 270336000 | bytes 4719616 | tf_op jit(solution)/shard_map/dot_general | solution.py:90
  188.9 2.9 %fusion.2 = bf16[128,2048]{1,0:T(8,128)(2,1)} fusion(f32[128,2048]{1,0:T(8,128)S(1)} %fusion.1, bf16[64,8,2048]{2,1,0:T(8,128)(2,1)} %all-to-all-done.1, f32[128]{0:T(128)S(1)} %get-tuple-element.29, s32[128]{0:T(128)S(1)} %get-tuple-element.27), kind=kOutput, calls=%fused_computation.4 | convolution fusion | flops 269287424 | bytes 3671040 | tf_op jit(solution)/shard_map/dot_general | solution.py:90
  (49 shorter events, 3.9 us)
Async XLA Ops:
  0.6 37.1 %copy-start = (bf16[512,2048]{1,0:T(8,128)(2,1)S(1)}, bf16[512,2048]{1,0:T(8,128)(2,1)}, u32[]{:S(2)}) copy-start(bf16[512,2048]{1,0:T(8,128)(2,1)} %param.19) | copy-start | bytes 6291460
  1.5 32.5 %collective-permute-start = (f32[2,512]{1,0:T(2,128)S(1)}, f32[2,512]{1,0:T(2,128)S(1)}, u32[]{:S(2)}, u32[]{:S(2)}) collective-permute-start(f32[2,512]{1,0:T(2,128)S(1)} %convert_multiply_fusion.1), channel_id=1, source_target_pairs={{0,4},{4,8},{8,12},{12,16},{16,20},{20,24},{24,28},{28,32},{32,36}... | collective-permute-start | bytes 12296 | tf_op jit(solution)/shard_map/ppermute | solution.py:23
  3.4 33.5 %collective-permute-start.3 = (bf16[2048,256]{1,0:T(8,128)(2,1)}, bf16[2048,256]{1,0:T(8,128)(2,1)}, u32[]{:S(2)}, u32[]{:S(2)}) collective-permute-start(bf16[2048,256]{1,0:T(8,128)(2,1)} %bitcast.53), channel_id=1, source_target_pairs={{0,1},{1,0},{2,5},{3,4},{4,3},{5,2},{6,7},{7,6},{8,9},{9,8},{10,13... | collective-permute-start | bytes 3145736 | tf_op jit(solution)/shard_map/ppermute | solution.py:34
  5.0 35.2 %collective-permute-start.4 = (bf16[2048,256]{1,0:T(8,128)(2,1)}, bf16[2048,256]{1,0:T(8,128)(2,1)}, u32[]{:S(2)}, u32[]{:S(2)}) collective-permute-start(bf16[2048,256]{1,0:T(8,128)(2,1)} %bitcast.54), channel_id=1, source_target_pairs={{0,1},{1,0},{2,5},{3,4},{4,3},{5,2},{6,7},{7,6},{8,9},{9,8},{10,13... | collective-permute-start | bytes 3145736 | tf_op jit(solution)/shard_map/ppermute | solution.py:34
  5.5 38.1 %collective-permute-start.11 = (bf16[256,2048]{1,0:T(8,128)(2,1)}, bf16[256,2048]{1,0:T(8,128)(2,1)}, u32[]{:S(2)}, u32[]{:S(2)}) collective-permute-start(bf16[256,2048]{1,0:T(8,128)(2,1)} %bitcast.55), channel_id=1, source_target_pairs={{0,1},{1,0},{2,5},{3,4},{4,3},{5,2},{6,7},{7,6},{8,9},{9,8},{10,13... | collective-permute-start | bytes 3145736 | tf_op jit(solution)/shard_map/ppermute | solution.py:34
  11.7 65.8 %all-to-all-start = ((bf16[64,8,2048]{2,1,0:T(8,128)(2,1)}), bf16[64,8,2048]{2,1,0:T(8,128)(2,1)}, u32[]{:S(2)}, u32[]{:S(2)}) async-start(bf16[64,8,2048]{2,1,0:T(8,128)(2,1)} %bitcast.52), calls=%async_computation | async-start | bytes 4194304 | tf_op jit(solution)/shard_map/all_to_all | solution.py:74
  27.1 2.6 %copy-start.2 = (bf16[2048,256]{1,0:T(8,128)(2,1)S(1)}, bf16[2048,256]{1,0:T(8,128)(2,1)}, u32[]{:S(2)}) copy-start(bf16[2048,256]{1,0:T(8,128)(2,1)} %param.25) | copy-start | bytes 3145732
  27.1 4.0 %copy-start.1 = (bf16[256,2048]{1,0:T(8,128)(2,1)S(1)}, bf16[256,2048]{1,0:T(8,128)(2,1)}, u32[]{:S(2)}) copy-start(bf16[256,2048]{1,0:T(8,128)(2,1)} %param.27) | copy-start | bytes 3145732
  29.7 4.3 %copy-start.8 = (bf16[3,512]{1,0:T(4,128)(2,1)S(1)}, bf16[3,512]{1,0:T(4,128)(2,1)}, u32[]{:S(2)}) copy-start(bf16[3,512]{1,0:T(4,128)(2,1)} %param.18) | copy-start | bytes 9220
  37.0 22.6 %collective-permute-start.7 = (bf16[2048,256]{1,0:T(8,128)(2,1)}, bf16[2048,256]{1,0:T(8,128)(2,1)S(1)}, u32[]{:S(2)}, u32[]{:S(2)}) collective-permute-start(bf16[2048,256]{1,0:T(8,128)(2,1)} %collective-permute-done.3.refs_1_), channel_id=1, source_target_pairs={{2,3},{3,2},{4,5},{5,4},{10,11},{11,10},{12,13},{13,12},{18,19},{1... | collective-permute-start | bytes 3145736 | tf_op jit(solution)/shard_map/ppermute | solution.py:34
  40.2 19.7 %copy-start.4 = (bf16[1,2048,256]{2,1,0:T(8,128)(2,1)S(1)}, bf16[1,2048,256]{2,1,0:T(8,128)(2,1)}, u32[]{:S(2)}) copy-start(bf16[1,2048,256]{2,1,0:T(8,128)(2,1)} %param.22) | copy-start | bytes 3145732
  40.2 20.8 %collective-permute-start.8 = (bf16[2048,256]{1,0:T(8,128)(2,1)}, bf16[2048,256]{1,0:T(8,128)(2,1)S(1)}, u32[]{:S(2)}, u32[]{:S(2)}) collective-permute-start(bf16[2048,256]{1,0:T(8,128)(2,1)} %collective-permute-done.4.refs_2_), channel_id=1, source_target_pairs={{2,3},{3,2},{4,5},{5,4},{10,11},{11,10},{12,13},{13,12},{18,19},{1... | collective-permute-start | bytes 3145736 | tf_op jit(solution)/shard_map/ppermute | solution.py:34
  43.6 17.5 %copy-start.5 = (bf16[1,2048,256]{2,1,0:T(8,128)(2,1)S(1)}, bf16[1,2048,256]{2,1,0:T(8,128)(2,1)}, u32[]{:S(2)}) copy-start(bf16[1,2048,256]{2,1,0:T(8,128)(2,1)} %param.23) | copy-start | bytes 3145732
  43.6 21.2 %collective-permute-start.13 = (bf16[256,2048]{1,0:T(8,128)(2,1)}, bf16[256,2048]{1,0:T(8,128)(2,1)S(1)}, u32[]{:S(2)}, u32[]{:S(2)}) collective-permute-start(bf16[256,2048]{1,0:T(8,128)(2,1)} %collective-permute-done.11.refs_9_), channel_id=1, source_target_pairs={{2,3},{3,2},{4,5},{5,4},{10,11},{11,10},{12,13},{13,12},{18,19},{1... | collective-permute-start | bytes 3145736 | tf_op jit(solution)/shard_map/ppermute | solution.py:34
  44.5 31.6 %collective-permute-start.12 = (bf16[256,2048]{1,0:T(8,128)(2,1)}, bf16[256,2048]{1,0:T(8,128)(2,1)}, u32[]{:S(2)}, u32[]{:S(2)}) collective-permute-start(bf16[256,2048]{1,0:T(8,128)(2,1)} %collective-permute-done.11.refs_9_), channel_id=1, source_target_pairs={{0,4},{1,5},{2,6},{3,7},{4,0},{5,1},{6,2},{7,3},{8,12},{9,13},{10,... | collective-permute-start | bytes 3145736 | tf_op jit(solution)/shard_map/ppermute | solution.py:34
  59.4 18.0 %collective-permute-start.5 = (bf16[2048,256]{1,0:T(8,128)(2,1)}, bf16[2048,256]{1,0:T(8,128)(2,1)}, u32[]{:S(2)}, u32[]{:S(2)}) collective-permute-start(bf16[2048,256]{1,0:T(8,128)(2,1)} %collective-permute-done.3.refs_1_), channel_id=1, source_target_pairs={{0,4},{1,5},{2,6},{3,7},{4,0},{5,1},{6,2},{7,3},{8,12},{9,13},{10,... | collective-permute-start | bytes 3145736 | tf_op jit(solution)/shard_map/ppermute | solution.py:34
  59.5 17.9 %collective-permute-start.6 = (bf16[2048,256]{1,0:T(8,128)(2,1)}, bf16[2048,256]{1,0:T(8,128)(2,1)}, u32[]{:S(2)}, u32[]{:S(2)}) collective-permute-start(bf16[2048,256]{1,0:T(8,128)(2,1)} %collective-permute-done.4.refs_2_), channel_id=1, source_target_pairs={{0,4},{1,5},{2,6},{3,7},{4,0},{5,1},{6,2},{7,3},{8,12},{9,13},{10,... | collective-permute-start | bytes 3145736 | tf_op jit(solution)/shard_map/ppermute | solution.py:34
  61.1 3.7 %copy-start.6 = (bf16[1,256,2048]{2,1,0:T(8,128)(2,1)S(1)}, bf16[1,256,2048]{2,1,0:T(8,128)(2,1)}, u32[]{:S(2)}) copy-start(bf16[1,256,2048]{2,1,0:T(8,128)(2,1)} %param.24) | copy-start | bytes 3145732
  62.1 16.5 %collective-permute-start.10 = (bf16[2048,256]{1,0:T(8,128)(2,1)}, bf16[2048,256]{1,0:T(8,128)(2,1)}, u32[]{:S(2)}, u32[]{:S(2)}) collective-permute-start(bf16[2048,256]{1,0:T(8,128)(2,1)} %broadcast_select_fusion.1.refs_6_), channel_id=1, source_target_pairs={{0,4},{1,5},{2,6},{3,7},{4,0},{5,1},{6,2},{7,3},{8,12},{9,13},{10,... | collective-permute-start | bytes 3145736 | tf_op jit(solution)/shard_map/ppermute | solution.py:34
  65.9 12.8 %collective-permute-start.14 = (bf16[256,2048]{1,0:T(8,128)(2,1)}, bf16[256,2048]{1,0:T(8,128)(2,1)}, u32[]{:S(2)}, u32[]{:S(2)}) collective-permute-start(bf16[256,2048]{1,0:T(8,128)(2,1)} %broadcast_select_fusion.refs_11_), channel_id=1, source_target_pairs={{0,4},{1,5},{2,6},{3,7},{4,0},{5,1},{6,2},{7,3},{8,12},{9,13},{10,... | collective-permute-start | bytes 3145736 | tf_op jit(solution)/shard_map/ppermute | solution.py:34
  76.0 4.1 %collective-permute-start.9 = (bf16[2048,256]{1,0:T(8,128)(2,1)}, bf16[2048,256]{1,0:T(8,128)(2,1)}, u32[]{:S(2)}, u32[]{:S(2)}) collective-permute-start(bf16[2048,256]{1,0:T(8,128)(2,1)} %broadcast_select_fusion.2.refs_5_), channel_id=1, source_target_pairs={{0,4},{1,5},{2,6},{3,7},{4,0},{5,1},{6,2},{7,3},{8,12},{9,13},{10,... | collective-permute-start | bytes 3145736 | tf_op jit(solution)/shard_map/ppermute | solution.py:34
  90.7 94.8 %all-to-all-start.1 = ((bf16[64,8,2048]{2,1,0:T(8,128)(2,1)}), bf16[64,8,2048]{2,1,0:T(8,128)(2,1)}, u32[]{:S(2)}, u32[]{:S(2)}) async-start(bf16[64,8,2048]{2,1,0:T(8,128)(2,1)} %bitcast.51), calls=%async_computation.1 | async-start | bytes 4194304 | tf_op jit(solution)/shard_map/all_to_all | solution.py:74
  105.8 28.4 %collective-permute-start.18 = (bf16[128,2048]{1,0:T(8,128)(2,1)}, bf16[128,2048]{1,0:T(8,128)(2,1)}, u32[]{:S(2)}, u32[]{:S(2)}) collective-permute-start(bf16[128,2048]{1,0:T(8,128)(2,1)} %get-tuple-element.14), channel_id=1, source_target_pairs={{0,3},{1,2},{2,1},{3,0},{4,7},{5,6},{6,5},{7,4},{8,11},{9,10},{10,... | collective-permute-start | bytes 1572872 | tf_op jit(solution)/shard_map/ppermute | solution.py:15
  108.5 25.7 %collective-permute-start.16 = (bf16[128,2048]{1,0:T(8,128)(2,1)}, bf16[128,2048]{1,0:T(8,128)(2,1)S(1)}, u32[]{:S(2)}, u32[]{:S(2)}) collective-permute-start(bf16[128,2048]{1,0:T(8,128)(2,1)} %get-tuple-element.14), channel_id=1, source_target_pairs={{0,1},{1,0},{2,3},{3,2},{4,5},{5,4},{6,7},{7,6},{8,9},{9,8},{10,11... | collective-permute-start | bytes 1572872 | tf_op jit(solution)/shard_map/ppermute | solution.py:15
  109.2 44.8 %collective-permute-start.2 = (bf16[128,2048]{1,0:T(8,128)(2,1)}, bf16[128,2048]{1,0:T(8,128)(2,1)}, u32[]{:S(2)}, u32[]{:S(2)}) collective-permute-start(bf16[128,2048]{1,0:T(8,128)(2,1)} %convolution_convert_fusion.4), channel_id=1, source_target_pairs={{0,3},{1,2},{2,1},{3,0},{4,7},{5,6},{6,5},{7,4},{8,11},{9,10},{10,... | collective-permute-start | bytes 1572872 | tf_op jit(solution)/shard_map/ppermute | solution.py:15
  109.8 65.1 %collective-permute-start.1 = (bf16[128,2048]{1,0:T(8,128)(2,1)}, bf16[128,2048]{1,0:T(8,128)(2,1)}, u32[]{:S(2)}, u32[]{:S(2)}) collective-permute-start(bf16[128,2048]{1,0:T(8,128)(2,1)} %convolution_convert_fusion.6), channel_id=1, source_target_pairs={{0,3},{1,2},{2,1},{3,0},{4,7},{5,6},{6,5},{7,4},{8,11},{9,10},{10,... | collective-permute-start | bytes 1572872 | tf_op jit(solution)/shard_map/ppermute | solution.py:15
  134.2 15.1 %collective-permute-start.19 = (bf16[128,2048]{1,0:T(8,128)(2,1)}, bf16[128,2048]{1,0:T(8,128)(2,1)}, u32[]{:S(2)}, u32[]{:S(2)}) collective-permute-start(bf16[128,2048]{1,0:T(8,128)(2,1)} %collective-permute-done.18), channel_id=1, source_target_pairs={{0,1},{1,0},{2,3},{3,2},{4,5},{5,4},{6,7},{7,6},{8,9},{9,8},{10,11... | collective-permute-start | bytes 1572872 | tf_op jit(solution)/shard_map/ppermute | solution.py:15
  134.2 0.8 copy-start.3
  139.5 42.1 %collective-permute-start.17 = (bf16[128,2048]{1,0:T(8,128)(2,1)}, bf16[128,2048]{1,0:T(8,128)(2,1)}, u32[]{:S(2)}, u32[]{:S(2)}) collective-permute-start(bf16[128,2048]{1,0:T(8,128)(2,1)} %convolution_convert_fusion.2), channel_id=1, source_target_pairs={{0,1},{1,0},{2,3},{3,2},{4,5},{5,4},{6,7},{7,6},{8,9},{9,8},{10,11... | collective-permute-start | bytes 1572872 | tf_op jit(solution)/shard_map/ppermute | solution.py:15
  154.0 17.8 %collective-permute-start.20 = (bf16[128,2048]{1,0:T(8,128)(2,1)}, bf16[128,2048]{1,0:T(8,128)(2,1)}, u32[]{:S(2)}, u32[]{:S(2)}) collective-permute-start(bf16[128,2048]{1,0:T(8,128)(2,1)} %convolution_convert_fusion), channel_id=1, source_target_pairs={{0,1},{1,0},{2,3},{3,2},{4,5},{5,4},{6,7},{7,6},{8,9},{9,8},{10,11... | collective-permute-start | bytes 1572872 | tf_op jit(solution)/shard_map/ppermute | solution.py:15
  156.1 23.1 %collective-permute-start.15 = (bf16[128,2048]{1,0:T(8,128)(2,1)}, bf16[128,2048]{1,0:T(8,128)(2,1)}, u32[]{:S(2)}, u32[]{:S(2)}) collective-permute-start(bf16[128,2048]{1,0:T(8,128)(2,1)} %add_convert_fusion.2), channel_id=1, source_target_pairs={{0,1},{1,0},{2,3},{3,2},{4,5},{5,4},{6,7},{7,6},{8,9},{9,8},{10,11... | collective-permute-start | bytes 1572872 | tf_op jit(solution)/shard_map/ppermute | solution.py:15
  159.9 15.0 %copy-start.9 = (s32[2,128]{1,0:T(2,128)S(1)}, s32[2,128]{1,0:T(2,128)}, u32[]{:S(2)}) copy-start(s32[2,128]{1,0:T(2,128)} %get-tuple-element.23) | copy-start | bytes 3076
  174.9 10.6 %collective-permute-start.21 = (bf16[128,2048]{1,0:T(8,128)(2,1)}, bf16[128,2048]{1,0:T(8,128)(2,1)S(1)}, u32[]{:S(2)}, u32[]{:S(2)}) collective-permute-start(bf16[128,2048]{1,0:T(8,128)(2,1)} %add_convert_fusion), channel_id=1, source_target_pairs={{0,3},{1,2},{2,1},{3,0},{4,7},{5,6},{6,5},{7,4},{8,11},{9,10},{10,... | collective-permute-start | bytes 1572872 | tf_op jit(solution)/shard_map/ppermute | solution.py:15
  185.5 0.8 copy-start.7

commit v3 on v2

--- a/solution.py
+++ b/solution.py
@@ -191,6 +191,32 @@
     )(moe_input, norm_gain.reshape(1, width), routes.T)
 
 
+def combine_kernel(slots_ref, weights_ref, rows_ref, *refs):
+    parts, out_ref = refs[:-1], refs[-1]
+    total = sum(part[...].astype(jnp.float32) for part in parts)
+    slot_ids = lax.broadcasted_iota(jnp.int32, (out_ref.shape[0], rows_ref.shape[0]), 1)
+    for k in range(slots_ref.shape[1]):
+        picks = jnp.where(slot_ids == slots_ref[:, k : k + 1], 1.0, 0.0).astype(rows_ref.dtype)
+        total = total + dot(picks, rows_ref[...]) * weights_ref[:, k : k + 1]
+    out_ref[...] = total.astype(out_ref.dtype)
+
+
+def combined(rows, slots, weights, parts, tiles=4):
+    count, width = rows.shape
+    tokens, top = slots.shape
+    small = pl.BlockSpec((tokens, top), lambda j: (0, 0))
+    tile = pl.BlockSpec((tokens, width // tiles), lambda j: (0, j))
+    return pl.pallas_call(
+        combine_kernel,
+        grid=(tiles,),
+        out_shape=jax.ShapeDtypeStruct((tokens, width), jnp.bfloat16),
+        in_specs=[small, small, pl.BlockSpec((count, width // tiles), lambda j: (0, j))]
+        + [tile] * len(parts),
+        out_specs=tile,
+        name="combined",
+    )(slots, weights, rows, *parts)
+
+
 def per_device(
     outer_gate,
     inner_gate,
@@ -259,13 +285,11 @@
     def shared_part(rows):
         return dot(swiglu(rows, shared_gate, shared_up), shared_down).astype(jnp.bfloat16)
 
-    normed_across = across(normed)
-    normed_beside = beside(normed)
     shared = {"own": shared_part(normed)}
     early = (*mix.values(), *shared.values())
     spread("gate", *early)
     spread("up", second["gate"])
-    spread("down", second["up"])
+    spread("down", fourth["up"])
 
     landed = after(landed, *early)
     blocks = (first, third, second, fourth)
@@ -274,27 +298,26 @@
     returned = exchanged(total.reshape(ep_count, capacity, model_width))
     returned = returned.reshape(slot_rows, model_width)
 
+    normed_across = across(normed)
+    normed_beside = beside(normed)
     normed_far = beside(normed_across)
 
     got_own = across(mix["across"])
     got_beside = after(across(mix["far"]), total)
-    got_rest = beside(both(mix["beside"], got_beside).astype(jnp.bfloat16))
+    mix_sum = both(mix["beside"], got_beside).astype(jnp.bfloat16)
+    got_rest = beside(mix_sum)
     mixer_out = both(mix["own"], got_own) + got_rest.astype(jnp.float32)
 
-    shared["far"] = shared_part(after(normed_far, total))
-    shared["beside"] = shared_part(after(normed_beside, total))
-    shared["across"] = shared_part(after(normed_across, total))
+    shared["far"] = shared_part(after(normed_far, mix_sum))
+    shared["across"] = shared_part(after(normed_across, shared["far"]))
+    shared["beside"] = shared_part(after(normed_beside, shared["far"]))
+    got_own = beside(shared["beside"])
     got_across = beside(shared["far"])
-    got_own = beside(shared["beside"])
-    got_rest = across(both(shared["across"], got_across).astype(jnp.bfloat16))
-    shared_total = both(shared["own"], got_own) + got_rest.astype(jnp.float32)
-
-    slot_ids = lax.broadcasted_iota(jnp.int32, (own_rows, slot_rows), 1)
-    routed = shared_total
-    for choice in range(top_count):
-        picks = (slot_ids == slots[:, choice][:, None]).astype(jnp.bfloat16)
-        routed = routed + dot(picks, returned) * own_weights[:, choice][:, None]
-    return (mixer_out.astype(jnp.bfloat16), routed.astype(jnp.bfloat16))
+    passed_on = both(shared["across"], got_across).astype(jnp.bfloat16)
+    shared_parts = (shared["own"], got_own, across(passed_on))
+
+    expert_mix = combined(returned, slots, own_weights, shared_parts)
+    return (mixer_out.astype(jnp.bfloat16), expert_mix)
 
 
 def solution(mesh):

time: 193 us -> 203 us (1.052)
  waiting for transfers between devices: 53.7 us -> 64.4 us
  matrix products: 28.8 us -> 23.3 us
  Pallas kernels: 13.8 us -> 18.3 us
  starting transfers between devices: 76.7 us -> 74.1 us
  local copies, waits for them, and re-layouts: 3.63 us -> 6.03 us
    ppermute x9, waiting for transfers between devices: 49.6 us -> 61.4 us  [swapped(): lax.ppermute(array, axis, [(i, partner(i)) for i in range(lax.axis_size(a...]
    dot_general x14 -> x12, matrix products: 28.8 us -> 23.3 us  [dot(): return jnp.dot(left, right, preferred_element_type=jnp.float32)]
    pallas_call x0 -> x1, Pallas kernels: none -> 4.46 us  [combined(): pl.pallas_call(combine_kernel, grid=(tiles,), out_shape=jax.ShapeDtypeStr...]
    ppermute x9, starting transfers between devices: 10.1 us -> 7.47 us  [swapped(): lax.ppermute(array, axis, [(i, partner(i)) for i in range(lax.axis_size(a...]
  transfers between devices with their start and end apart: 24 -> 24, of which waited for: 8 -> 8; matrix products, arithmetic and copies ran while one was open for 20% -> 19% of each run, Pallas kernels for 2% -> 2%
where the time goes in v3:
time: 203 us; the launch traced here: 200 us
  starting transfers between devices  74.1 us (37%)
  waiting for transfers between devices  64.4 us (32%)
  matrix products  23.3 us (11%)
  Pallas kernels  18.3 us (9%)
  other arithmetic  13 us (6%)
  local copies, waits for them, and re-layouts  6.03 us (3%)
    ppermute x9, waiting for transfers between devices, swapped(): lax.ppermute(array, axis, [(i, partner(i)) for i in range(lax.axis_size(a...  61.4 us
    ppermute x12, starting transfers between devices, moved(): return lax.ppermute(block, ('ep', 'tp'), route)  34.3 us
    all_to_all x2, starting transfers between devices, exchanged(): lax.all_to_all(blocks, ('ep', 'tp'), 0, 0, axis_index_groups=groups, tile...  30.5 us
    dot_general x12, matrix products, dot(): return jnp.dot(left, right, preferred_element_type=jnp.float32)  23.3 us
    pallas_call x1, Pallas kernels, expert(): pl.pallas_call(partial(expert_kernel, count=count), out_shape=jax.ShapeDt...  10.5 us
    ppermute x9, starting transfers between devices, swapped(): lax.ppermute(array, axis, [(i, partner(i)) for i in range(lax.axis_size(a...  7.47 us
    pallas_call x1, Pallas kernels, combined(): pl.pallas_call(combine_kernel, grid=(tiles,), out_shape=jax.ShapeDtypeStr...  4.46 us
  transfers between devices with their start and end apart: 24, of which 8 were waited for; matrix products, arithmetic and copies ran while one was open for 19% of the time, Pallas kernels for 2%

profile of v3, /device:TPU:8, one launch (start us, length us, event | category | flops | bytes accessed | tf_op | source)
XLA Modules:
  0.0 200.1 jit_solution(10957244771960374654)
XLA Ops:
  0.6 0.9 convert_multiply_fusion.1
  1.5 1.9 collective-permute-start
  3.4 1.6 collective-permute-start.3
  5.5 1.5 collective-permute-start.11
  7.0 1.3 reshape.19.gain_ref
  8.3 3.3 %dispatched.1 = (bf16[128,2048]{1,0:T(8,128)(2,1)}, bf16[512,2048]{1,0:T(8,128)(2,1)}, s32[2,128]{1,0:T(2,128)}) custom-call(bf16[128,2048]{1,0:T(8,128)(2,1)} %x_ref.1, bf16[1,2048]{1,0:T(2,128)(2,1)} %reshape.19.gain_ref, s32[2,512]{1,0:T(2,128)} %bitcast.48), custom_call_target="tpu_custom_call" | custom-call | tf_op jit(solution)/shard_map/dispatched/pallas_call | solution.py:181
  11.7 15.4 %all-to-all-start = ((bf16[64,8,2048]{2,1,0:T(8,128)(2,1)}), bf16[64,8,2048]{2,1,0:T(8,128)(2,1)}, u32[]{:S(2)}, u32[]{:S(2)}) async-start(bf16[64,8,2048]{2,1,0:T(8,128)(2,1)} %bitcast.40), calls=%async_computation | async-start | bytes 4194304 | tf_op jit(solution)/shard_map/all_to_all | solution.py:74
  27.1 2.6 %convert_multiply_fusion = f32[512,512]{1,0:T(8,128)} fusion(bf16[512,512]{1,0:T(8,128)(2,1)} %param.17, bf16[512,512]{1,0:T(8,128)(2,1)} %param.16), kind=kLoop, calls=%fused_computation.24 | loop fusion | flops 786432 | bytes 2097152 | tf_op jit(solution)/shard_map/mul | solution.py:78
  29.7 1.4 fusion.37
  31.0 3.0 %convolution_convert_fusion.3.refs_0_ = bf16[128,2048]{1,0:T(8,128)(2,1)} fusion(bf16[256,2048]{1,0:T(8,128)(2,1)S(1)} %copy-done.1, bf16[128,2048]{1,0:T(8,128)(2,1)} %get-tuple-element.14, bf16[2048,256]{1,0:T(8,128)(2,1)} %param.26, f32[128,256]{1,0:T(8,128)S(1)} %fusion.37), kind=kOutput, calls=%fused_computation.4 | convolution fusion | flops 268894208 | bytes 3276800 | tf_op jit(solution)/shard_map/dot_general | solution.py:90
  34.1 2.9 %fusion.7 = bf16[512,512]{1,0:T(8,128)(2,1)S(1)} fusion(f32[2,512]{1,0:T(2,128)S(1)} %collective-permute-done, f32[512,512]{1,0:T(8,128)} %convert_multiply_fusion, bf16[512,512]{1,0:T(8,128)(2,1)} %param.15, f32[512]{0:T(512)S(1)} %bitcast.47, f32[512]{0:T(512)S(1)} %bitcast.46, f32[512]{0:T(512)S(1)} %bitcast.45), kind=kLoop, calls=%fused_computation.18 | loop fusion | flops 2621440 | bytes 2107392 | tf_op jit(solution)/shard_map/convert_element_type | solution.py:278
  37.0 0.7 collective-permute-start.7
  37.7 1.3 convolution_convert_fusion.6
  39.0 1.2 convolution_convert_fusion.4
  40.2 0.8 collective-permute-start.8
  41.1 1.2 convolution_convert_fusion.7
  42.4 1.2 convolution_convert_fusion.5
  43.6 0.8 collective-permute-start.13
  44.5 1.1 broadcast_select_fusion.2.refs_5_
  45.7 1.0 copy-done.3
  46.7 18.1 %collective-permute-start.10 = (bf16[2048,256]{1,0:T(8,128)(2,1)S(1)}, bf16[2048,256]{1,0:T(8,128)(2,1)}, u32[]{:S(2)}, u32[]{:S(2)}) collective-permute-start(bf16[2048,256]{1,0:T(8,128)(2,1)S(1)} %broadcast_select_fusion.1.refs_6_), channel_id=1, source_target_pairs={{0,4},{1,5},{2,6},{3,7},{4,0},{5,1},{6,2},{7,3},{8,12},{9,13},{10,... | collective-permute-start | bytes 3145736 | tf_op jit(solution)/shard_map/ppermute | solution.py:34
  65.3 9.6 %collective-permute-start.9 = (bf16[2048,256]{1,0:T(8,128)(2,1)}, bf16[2048,256]{1,0:T(8,128)(2,1)}, u32[]{:S(2)}, u32[]{:S(2)}) collective-permute-start(bf16[2048,256]{1,0:T(8,128)(2,1)} %broadcast_select_fusion.2.refs_5_), channel_id=1, source_target_pairs={{0,4},{1,5},{2,6},{3,7},{4,0},{5,1},{6,2},{7,3},{8,12},{9,13},{10,... | collective-permute-start | bytes 3145736 | tf_op jit(solution)/shard_map/ppermute | solution.py:34
  74.9 1.1 broadcast_select_fusion.refs_11_
  76.0 1.4 all-to-all-done
  77.6 1.5 collective-permute-done.14.refs_12_
  79.1 10.5 %expert.1 = bf16[512,2048]{1,0:T(8,128)(2,1)} custom-call(bf16[512,2048]{1,0:T(8,128)(2,1)} %bitcast.5.refs_0_, bf16[2048,256]{1,0:T(8,128)(2,1)} %collective-permute-done.3.refs_1_, bf16[2048,256]{1,0:T(8,128)(2,1)} %collective-permute-done.4.refs_2_, bf16[2048,256]{1,0:T(8,128)(2,1)} %collective-permute-done.5.refs_3_, ...), custom_call_target="tpu_custom_call" | custom-call | tf_op jit(solution)/shard_map/expert/pallas_call | solution.py:132
  89.6 15.1 %all-to-all-start.1 = ((bf16[64,8,2048]{2,1,0:T(8,128)(2,1)}), bf16[64,8,2048]{2,1,0:T(8,128)(2,1)}, u32[]{:S(2)}, u32[]{:S(2)}) async-start(bf16[64,8,2048]{2,1,0:T(8,128)(2,1)} %bitcast.39), calls=%async_computation.1 | async-start | bytes 4194304 | tf_op jit(solution)/shard_map/all_to_all | solution.py:74
  104.7 2.8 %collective-permute-start.17 = (bf16[128,2048]{1,0:T(8,128)(2,1)}, bf16[128,2048]{1,0:T(8,128)(2,1)S(1)}, u32[]{:S(2)}, u32[]{:S(2)}) collective-permute-start(bf16[128,2048]{1,0:T(8,128)(2,1)} %get-tuple-element.14), channel_id=1, source_target_pairs={{0,3},{1,2},{2,1},{3,0},{4,7},{5,6},{6,5},{7,4},{8,11},{9,10},{10,... | collective-permute-start | bytes 1572872 | tf_op jit(solution)/shard_map/ppermute | solution.py:15
  108.0 25.0 %collective-permute-done.17 = bf16[128,2048]{1,0:T(8,128)(2,1)S(1)} collective-permute-done((bf16[128,2048]{1,0:T(8,128)(2,1)}, bf16[128,2048]{1,0:T(8,128)(2,1)S(1)}, u32[]{:S(2)}, u32[]{:S(2)}) %collective-permute-start.17) | collective-permute-done | bytes 524320 | tf_op jit(solution)/shard_map/ppermute | solution.py:15
  133.0 2.0 %collective-permute-start.16 = (bf16[128,2048]{1,0:T(8,128)(2,1)}, bf16[128,2048]{1,0:T(8,128)(2,1)}, u32[]{:S(2)}, u32[]{:S(2)}) collective-permute-start(bf16[128,2048]{1,0:T(8,128)(2,1)} %get-tuple-element.14), channel_id=1, source_target_pairs={{0,1},{1,0},{2,3},{3,2},{4,5},{5,4},{6,7},{7,6},{8,9},{9,8},{10,11... | collective-permute-start | bytes 1572872 | tf_op jit(solution)/shard_map/ppermute | solution.py:15
  135.0 17.8 %collective-permute-done.2 = bf16[128,2048]{1,0:T(8,128)(2,1)S(1)} collective-permute-done((bf16[128,2048]{1,0:T(8,128)(2,1)}, bf16[128,2048]{1,0:T(8,128)(2,1)S(1)}, u32[]{:S(2)}, u32[]{:S(2)}) %collective-permute-start.2) | collective-permute-done | bytes 524320 | tf_op jit(solution)/shard_map/ppermute | solution.py:15
  152.8 2.0 add_convert_fusion.2
  154.8 0.8 copy-done.4
  155.6 1.5 fusion.38
  157.1 3.0 %convolution_convert_fusion.2 = bf16[128,2048]{1,0:T(8,128)(2,1)} fusion(bf16[256,2048]{1,0:T(8,128)(2,1)S(1)} %copy-done.1, f32[128,256]{1,0:T(8,128)S(1)} %fusion.38, bf16[128,2048]{1,0:T(8,128)(2,1)} %copy-done.4, bf16[2048,256]{1,0:T(8,128)(2,1)} %param.26), kind=kOutput, calls=%fused_computation.3 | convolution fusion | flops 268894208 | bytes 3276800 | tf_op jit(solution)/shard_map/dot_general | solution.py:90
  160.1 2.0 %collective-permute-start.20 = (bf16[128,2048]{1,0:T(8,128)(2,1)}, bf16[128,2048]{1,0:T(8,128)(2,1)}, u32[]{:S(2)}, u32[]{:S(2)}) collective-permute-start(bf16[128,2048]{1,0:T(8,128)(2,1)} %convolution_convert_fusion.2), channel_id=1, source_target_pairs={{0,1},{1,0},{2,3},{3,2},{4,5},{5,4},{6,7},{7,6},{8,9},{9,8},{10,11... | collective-permute-start | bytes 1572872 | tf_op jit(solution)/shard_map/ppermute | solution.py:15
  162.1 1.7 fusion.39
  163.8 3.0 %convolution_convert_fusion.1 = bf16[128,2048]{1,0:T(8,128)(2,1)} fusion(bf16[256,2048]{1,0:T(8,128)(2,1)S(1)} %copy-done.1, f32[128,256]{1,0:T(8,128)S(1)} %fusion.39, bf16[128,2048]{1,0:T(8,128)(2,1)} %collective-permute-done.16, bf16[2048,256]{1,0:T(8,128)(2,1)} %param.26), kind=kOutput, calls=%fused_computation.2 | convolution fusion | flops 268894208 | bytes 3276800 | tf_op jit(solution)/shard_map/dot_general | solution.py:90
  166.7 1.7 fusion.40
  168.6 12.5 %collective-permute-done.20 = bf16[128,2048]{1,0:T(8,128)(2,1)} collective-permute-done((bf16[128,2048]{1,0:T(8,128)(2,1)}, bf16[128,2048]{1,0:T(8,128)(2,1)}, u32[]{:S(2)}, u32[]{:S(2)}) %collective-permute-start.20) | collective-permute-done | bytes 524320 | tf_op jit(solution)/shard_map/ppermute | solution.py:15
  181.1 3.1 %add_convert_fusion = bf16[128,2048]{1,0:T(8,128)(2,1)} fusion(bf16[128,2048]{1,0:T(8,128)(2,1)} %collective-permute-done.20, bf16[256,2048]{1,0:T(8,128)(2,1)S(1)} %copy-done.1, f32[128,256]{1,0:T(8,128)S(1)} %fusion.40, bf16[128,2048]{1,0:T(8,128)(2,1)} %copy-done.5, bf16[2048,256]{1,0:T(8,128)(2,1)} %param.26), kind=kOutput, calls=%fused_computation.21 | convolution fusion | flops 269942784 | bytes 3801088 | tf_op jit(solution)/shard_map/dot_general | solution.py:90
  184.2 0.7 constant_dynamic-slice_fusion
  184.9 0.7 copy.19.weights_ref
  185.6 0.7 copy.17
  186.3 2.4 %add_convert_fusion.1 = bf16[128,2048]{1,0:T(8,128)(2,1)} fusion(bf16[128,2048]{1,0:T(8,128)(2,1)} %collective-permute-done.15, bf16[128,2048]{1,0:T(8,128)(2,1)} %collective-permute-done.1, bf16[128,2048]{1,0:T(8,128)(2,1)} %convolution_convert_fusion.7), kind=kLoop, calls=%fused_computation.22 | loop fusion | flops 1572864 | bytes 2097152 | tf_op jit(solution)/shard_map/convert_element_type | solution.py:320
  189.2 5.6 %collective-permute-done.21.refs_2_ = bf16[128,2048]{1,0:T(8,128)(2,1)S(1)} collective-permute-done((bf16[128,2048]{1,0:T(8,128)(2,1)}, bf16[128,2048]{1,0:T(8,128)(2,1)S(1)}, u32[]{:S(2)}, u32[]{:S(2)}) %collective-permute-start.21) | collective-permute-done | bytes 524320 | tf_op jit(solution)/shard_map/ppermute | solution.py:15
  194.8 0.8 copy-done.9
  195.6 4.5 %combined.1 = bf16[128,2048]{1,0:T(8,128)(2,1)} custom-call(s32[128,2]{1,0:T(8,128)} %bitcast.44, f32[128,2]{1,0:T(8,128)} %copy.19.weights_ref, bf16[512,2048]{1,0:T(8,128)(2,1)} %bitcast.11.rows_ref, bf16[128,2048]{1,0:T(8,128)(2,1)} %convolution_convert_fusion.3.refs_0_, bf16[128,2048]{1,0:T(8,128)(2,1)} %collective-permute-done.19.refs_1_, ...), custom_call_target="tpu_custom_call" | custom-call | tf_op jit(solution)/shard_map/combined/pallas_call | solution.py:209
  (52 shorter events, 2.5 us)
Async XLA Ops:
  0.6 37.1 %copy-start = (bf16[512,2048]{1,0:T(8,128)(2,1)S(1)}, bf16[512,2048]{1,0:T(8,128)(2,1)}, u32[]{:S(2)}) copy-start(bf16[512,2048]{1,0:T(8,128)(2,1)} %param.19) | copy-start | bytes 6291460
  1.5 32.5 %collective-permute-start = (f32[2,512]{1,0:T(2,128)S(1)}, f32[2,512]{1,0:T(2,128)S(1)}, u32[]{:S(2)}, u32[]{:S(2)}) collective-permute-start(f32[2,512]{1,0:T(2,128)S(1)} %convert_multiply_fusion.1), channel_id=1, source_target_pairs={{0,4},{4,8},{8,12},{12,16},{16,20},{20,24},{24,28},{28,32},{32,36}... | collective-permute-start | bytes 12296 | tf_op jit(solution)/shard_map/ppermute | solution.py:23
  3.4 33.5 %collective-permute-start.3 = (bf16[2048,256]{1,0:T(8,128)(2,1)}, bf16[2048,256]{1,0:T(8,128)(2,1)}, u32[]{:S(2)}, u32[]{:S(2)}) collective-permute-start(bf16[2048,256]{1,0:T(8,128)(2,1)} %bitcast.41), channel_id=1, source_target_pairs={{0,1},{1,0},{2,5},{3,4},{4,3},{5,2},{6,7},{7,6},{8,9},{9,8},{10,13... | collective-permute-start | bytes 3145736 | tf_op jit(solution)/shard_map/ppermute | solution.py:34
  5.0 35.2 %collective-permute-start.4 = (bf16[2048,256]{1,0:T(8,128)(2,1)}, bf16[2048,256]{1,0:T(8,128)(2,1)}, u32[]{:S(2)}, u32[]{:S(2)}) collective-permute-start(bf16[2048,256]{1,0:T(8,128)(2,1)} %bitcast.42), channel_id=1, source_target_pairs={{0,1},{1,0},{2,5},{3,4},{4,3},{5,2},{6,7},{7,6},{8,9},{9,8},{10,13... | collective-permute-start | bytes 3145736 | tf_op jit(solution)/shard_map/ppermute | solution.py:34
  5.5 38.1 %collective-permute-start.11 = (bf16[256,2048]{1,0:T(8,128)(2,1)}, bf16[256,2048]{1,0:T(8,128)(2,1)}, u32[]{:S(2)}, u32[]{:S(2)}) collective-permute-start(bf16[256,2048]{1,0:T(8,128)(2,1)} %bitcast.43), channel_id=1, source_target_pairs={{0,1},{1,0},{2,5},{3,4},{4,3},{5,2},{6,7},{7,6},{8,9},{9,8},{10,13... | collective-permute-start | bytes 3145736 | tf_op jit(solution)/shard_map/ppermute | solution.py:34
  11.7 65.8 %all-to-all-start = ((bf16[64,8,2048]{2,1,0:T(8,128)(2,1)}), bf16[64,8,2048]{2,1,0:T(8,128)(2,1)}, u32[]{:S(2)}, u32[]{:S(2)}) async-start(bf16[64,8,2048]{2,1,0:T(8,128)(2,1)} %bitcast.40), calls=%async_computation | async-start | bytes 4194304 | tf_op jit(solution)/shard_map/all_to_all | solution.py:74
  27.1 2.6 %copy-start.2 = (bf16[2048,256]{1,0:T(8,128)(2,1)S(1)}, bf16[2048,256]{1,0:T(8,128)(2,1)}, u32[]{:S(2)}) copy-start(bf16[2048,256]{1,0:T(8,128)(2,1)} %param.25) | copy-start | bytes 3145732
  27.1 4.0 %copy-start.1 = (bf16[256,2048]{1,0:T(8,128)(2,1)S(1)}, bf16[256,2048]{1,0:T(8,128)(2,1)}, u32[]{:S(2)}) copy-start(bf16[256,2048]{1,0:T(8,128)(2,1)} %param.27) | copy-start | bytes 3145732
  29.7 4.3 %copy-start.10 = (bf16[3,512]{1,0:T(4,128)(2,1)S(1)}, bf16[3,512]{1,0:T(4,128)(2,1)}, u32[]{:S(2)}) copy-start(bf16[3,512]{1,0:T(4,128)(2,1)} %param.18) | copy-start | bytes 9220
  37.0 7.5 %collective-permute-start.7 = (bf16[2048,256]{1,0:T(8,128)(2,1)}, bf16[2048,256]{1,0:T(8,128)(2,1)S(1)}, u32[]{:S(2)}, u32[]{:S(2)}) collective-permute-start(bf16[2048,256]{1,0:T(8,128)(2,1)} %collective-permute-done.3.refs_1_), channel_id=1, source_target_pairs={{2,3},{3,2},{4,5},{5,4},{10,11},{11,10},{12,13},{13,12},{18,19},{1... | collective-permute-start | bytes 3145736 | tf_op jit(solution)/shard_map/ppermute | solution.py:34
  40.2 4.2 %copy-start.6 = (bf16[1,2048,256]{2,1,0:T(8,128)(2,1)S(1)}, bf16[1,2048,256]{2,1,0:T(8,128)(2,1)}, u32[]{:S(2)}) copy-start(bf16[1,2048,256]{2,1,0:T(8,128)(2,1)} %param.22) | copy-start | bytes 3145732
  40.2 5.3 %collective-permute-start.8 = (bf16[2048,256]{1,0:T(8,128)(2,1)}, bf16[2048,256]{1,0:T(8,128)(2,1)S(1)}, u32[]{:S(2)}, u32[]{:S(2)}) collective-permute-start(bf16[2048,256]{1,0:T(8,128)(2,1)} %collective-permute-done.4.refs_2_), channel_id=1, source_target_pairs={{2,3},{3,2},{4,5},{5,4},{10,11},{11,10},{12,13},{13,12},{18,19},{1... | collective-permute-start | bytes 3145736 | tf_op jit(solution)/shard_map/ppermute | solution.py:34
  43.6 2.0 copy-start.7
  43.6 21.7 %collective-permute-start.13 = (bf16[256,2048]{1,0:T(8,128)(2,1)}, bf16[256,2048]{1,0:T(8,128)(2,1)S(1)}, u32[]{:S(2)}, u32[]{:S(2)}) collective-permute-start(bf16[256,2048]{1,0:T(8,128)(2,1)} %collective-permute-done.11.refs_9_), channel_id=1, source_target_pairs={{2,3},{3,2},{4,5},{5,4},{10,11},{11,10},{12,13},{13,12},{18,19},{1... | collective-permute-start | bytes 3145736 | tf_op jit(solution)/shard_map/ppermute | solution.py:34
  45.6 29.3 %copy-start.8 = (bf16[1,256,2048]{2,1,0:T(8,128)(2,1)S(1)}, bf16[1,256,2048]{2,1,0:T(8,128)(2,1)}, u32[]{:S(2)}) copy-start(bf16[1,256,2048]{2,1,0:T(8,128)(2,1)} %param.24) | copy-start | bytes 3145732
  45.7 1.0 copy-start.3
  46.7 28.3 %collective-permute-start.10 = (bf16[2048,256]{1,0:T(8,128)(2,1)S(1)}, bf16[2048,256]{1,0:T(8,128)(2,1)}, u32[]{:S(2)}, u32[]{:S(2)}) collective-permute-start(bf16[2048,256]{1,0:T(8,128)(2,1)S(1)} %broadcast_select_fusion.1.refs_6_), channel_id=1, source_target_pairs={{0,4},{1,5},{2,6},{3,7},{4,0},{5,1},{6,2},{7,3},{8,12},{9,13},{10,... | collective-permute-start | bytes 3145736 | tf_op jit(solution)/shard_map/ppermute | solution.py:34
  64.8 12.7 %collective-permute-start.12 = (bf16[256,2048]{1,0:T(8,128)(2,1)}, bf16[256,2048]{1,0:T(8,128)(2,1)}, u32[]{:S(2)}, u32[]{:S(2)}) collective-permute-start(bf16[256,2048]{1,0:T(8,128)(2,1)} %collective-permute-done.11.refs_9_), channel_id=1, source_target_pairs={{0,4},{1,5},{2,6},{3,7},{4,0},{5,1},{6,2},{7,3},{8,12},{9,13},{10,... | collective-permute-start | bytes 3145736 | tf_op jit(solution)/shard_map/ppermute | solution.py:34
  64.8 12.7 %collective-permute-start.5 = (bf16[2048,256]{1,0:T(8,128)(2,1)}, bf16[2048,256]{1,0:T(8,128)(2,1)}, u32[]{:S(2)}, u32[]{:S(2)}) collective-permute-start(bf16[2048,256]{1,0:T(8,128)(2,1)} %collective-permute-done.3.refs_1_), channel_id=1, source_target_pairs={{0,4},{1,5},{2,6},{3,7},{4,0},{5,1},{6,2},{7,3},{8,12},{9,13},{10,... | collective-permute-start | bytes 3145736 | tf_op jit(solution)/shard_map/ppermute | solution.py:34
  65.3 12.2 %collective-permute-start.6 = (bf16[2048,256]{1,0:T(8,128)(2,1)}, bf16[2048,256]{1,0:T(8,128)(2,1)}, u32[]{:S(2)}, u32[]{:S(2)}) collective-permute-start(bf16[2048,256]{1,0:T(8,128)(2,1)} %collective-permute-done.4.refs_2_), channel_id=1, source_target_pairs={{0,4},{1,5},{2,6},{3,7},{4,0},{5,1},{6,2},{7,3},{8,12},{9,13},{10,... | collective-permute-start | bytes 3145736 | tf_op jit(solution)/shard_map/ppermute | solution.py:34
  65.3 12.3 %collective-permute-start.9 = (bf16[2048,256]{1,0:T(8,128)(2,1)}, bf16[2048,256]{1,0:T(8,128)(2,1)}, u32[]{:S(2)}, u32[]{:S(2)}) collective-permute-start(bf16[2048,256]{1,0:T(8,128)(2,1)} %broadcast_select_fusion.2.refs_5_), channel_id=1, source_target_pairs={{0,4},{1,5},{2,6},{3,7},{4,0},{5,1},{6,2},{7,3},{8,12},{9,13},{10,... | collective-permute-start | bytes 3145736 | tf_op jit(solution)/shard_map/ppermute | solution.py:34
  76.0 3.0 %collective-permute-start.14 = (bf16[256,2048]{1,0:T(8,128)(2,1)}, bf16[256,2048]{1,0:T(8,128)(2,1)}, u32[]{:S(2)}, u32[]{:S(2)}) collective-permute-start(bf16[256,2048]{1,0:T(8,128)(2,1)} %broadcast_select_fusion.refs_11_), channel_id=1, source_target_pairs={{0,4},{1,5},{2,6},{3,7},{4,0},{5,1},{6,2},{7,3},{8,12},{9,13},{10,... | collective-permute-start | bytes 3145736 | tf_op jit(solution)/shard_map/ppermute | solution.py:34
  89.6 105.2 %all-to-all-start.1 = ((bf16[64,8,2048]{2,1,0:T(8,128)(2,1)}), bf16[64,8,2048]{2,1,0:T(8,128)(2,1)}, u32[]{:S(2)}, u32[]{:S(2)}) async-start(bf16[64,8,2048]{2,1,0:T(8,128)(2,1)} %bitcast.39), calls=%async_computation.1 | async-start | bytes 4194304 | tf_op jit(solution)/shard_map/all_to_all | solution.py:74
  104.7 28.3 %collective-permute-start.17 = (bf16[128,2048]{1,0:T(8,128)(2,1)}, bf16[128,2048]{1,0:T(8,128)(2,1)S(1)}, u32[]{:S(2)}, u32[]{:S(2)}) collective-permute-start(bf16[128,2048]{1,0:T(8,128)(2,1)} %get-tuple-element.14), channel_id=1, source_target_pairs={{0,3},{1,2},{2,1},{3,0},{4,7},{5,6},{6,5},{7,4},{8,11},{9,10},{10,... | collective-permute-start | bytes 1572872 | tf_op jit(solution)/shard_map/ppermute | solution.py:15
  107.4 45.4 %collective-permute-start.2 = (bf16[128,2048]{1,0:T(8,128)(2,1)}, bf16[128,2048]{1,0:T(8,128)(2,1)S(1)}, u32[]{:S(2)}, u32[]{:S(2)}) collective-permute-start(bf16[128,2048]{1,0:T(8,128)(2,1)} %convolution_convert_fusion.4), channel_id=1, source_target_pairs={{0,3},{1,2},{2,1},{3,0},{4,7},{5,6},{6,5},{7,4},{8,11},{9,10},{10,... | collective-permute-start | bytes 1572872 | tf_op jit(solution)/shard_map/ppermute | solution.py:15
  133.0 21.8 %copy-start.5 = (bf16[128,2048]{1,0:T(8,128)(2,1)}, bf16[128,2048]{1,0:T(8,128)(2,1)S(1)}, u32[]{:S(2)}) copy-start(bf16[128,2048]{1,0:T(8,128)(2,1)S(1)} %collective-permute-done.17) | copy-start | bytes 1572868
  133.0 21.8 %collective-permute-start.18 = (bf16[128,2048]{1,0:T(8,128)(2,1)S(1)}, bf16[128,2048]{1,0:T(8,128)(2,1)S(1)}, u32[]{:S(2)}, u32[]{:S(2)}) collective-permute-start(bf16[128,2048]{1,0:T(8,128)(2,1)S(1)} %collective-permute-done.17), channel_id=1, source_target_pairs={{0,1},{1,0},{2,3},{3,2},{4,5},{5,4},{6,7},{7,6},{8,9},{9,8},{10,11... | collective-permute-start | bytes 1572872 | tf_op jit(solution)/shard_map/ppermute | solution.py:15
  133.0 29.1 %collective-permute-start.16 = (bf16[128,2048]{1,0:T(8,128)(2,1)}, bf16[128,2048]{1,0:T(8,128)(2,1)}, u32[]{:S(2)}, u32[]{:S(2)}) collective-permute-start(bf16[128,2048]{1,0:T(8,128)(2,1)} %get-tuple-element.14), channel_id=1, source_target_pairs={{0,1},{1,0},{2,3},{3,2},{4,5},{5,4},{6,7},{7,6},{8,9},{9,8},{10,11... | collective-permute-start | bytes 1572872 | tf_op jit(solution)/shard_map/ppermute | solution.py:15
  135.0 51.3 %collective-permute-start.1 = (bf16[128,2048]{1,0:T(8,128)(2,1)}, bf16[128,2048]{1,0:T(8,128)(2,1)}, u32[]{:S(2)}, u32[]{:S(2)}) collective-permute-start(bf16[128,2048]{1,0:T(8,128)(2,1)} %convolution_convert_fusion.6), channel_id=1, source_target_pairs={{0,3},{1,2},{2,1},{3,0},{4,7},{5,6},{6,5},{7,4},{8,11},{9,10},{10,... | collective-permute-start | bytes 1572872 | tf_op jit(solution)/shard_map/ppermute | solution.py:15
  154.7 31.6 %collective-permute-start.15 = (bf16[128,2048]{1,0:T(8,128)(2,1)}, bf16[128,2048]{1,0:T(8,128)(2,1)}, u32[]{:S(2)}, u32[]{:S(2)}) collective-permute-start(bf16[128,2048]{1,0:T(8,128)(2,1)} %add_convert_fusion.2), channel_id=1, source_target_pairs={{0,1},{1,0},{2,3},{3,2},{4,5},{5,4},{6,7},{7,6},{8,9},{9,8},{10,11... | collective-permute-start | bytes 1572872 | tf_op jit(solution)/shard_map/ppermute | solution.py:15
  154.8 0.8 copy-start.4
  160.1 21.0 %collective-permute-start.20 = (bf16[128,2048]{1,0:T(8,128)(2,1)}, bf16[128,2048]{1,0:T(8,128)(2,1)}, u32[]{:S(2)}, u32[]{:S(2)}) collective-permute-start(bf16[128,2048]{1,0:T(8,128)(2,1)} %convolution_convert_fusion.2), channel_id=1, source_target_pairs={{0,1},{1,0},{2,3},{3,2},{4,5},{5,4},{6,7},{7,6},{8,9},{9,8},{10,11... | collective-permute-start | bytes 1572872 | tf_op jit(solution)/shard_map/ppermute | solution.py:15
  168.4 17.2 %copy-start.11 = (s32[2,128]{1,0:T(2,128)S(1)}, s32[2,128]{1,0:T(2,128)}, u32[]{:S(2)}) copy-start(s32[2,128]{1,0:T(2,128)} %get-tuple-element.20) | copy-start | bytes 3076
  168.5 20.7 %collective-permute-start.19 = (bf16[128,2048]{1,0:T(8,128)(2,1)}, bf16[128,2048]{1,0:T(8,128)(2,1)}, u32[]{:S(2)}, u32[]{:S(2)}) collective-permute-start(bf16[128,2048]{1,0:T(8,128)(2,1)} %convolution_convert_fusion.1), channel_id=1, source_target_pairs={{0,1},{1,0},{2,3},{3,2},{4,5},{5,4},{6,7},{7,6},{8,9},{9,8},{10,11... | collective-permute-start | bytes 1572872 | tf_op jit(solution)/shard_map/ppermute | solution.py:15
  184.2 10.6 %collective-permute-start.21 = (bf16[128,2048]{1,0:T(8,128)(2,1)}, bf16[128,2048]{1,0:T(8,128)(2,1)S(1)}, u32[]{:S(2)}, u32[]{:S(2)}) collective-permute-start(bf16[128,2048]{1,0:T(8,128)(2,1)} %add_convert_fusion), channel_id=1, source_target_pairs={{0,3},{1,2},{2,1},{3,0},{4,7},{5,6},{6,5},{7,4},{8,11},{9,10},{10,... | collective-permute-start | bytes 1572872 | tf_op jit(solution)/shard_map/ppermute | solution.py:15
  194.8 0.8 copy-start.9
